TPU v7x, 32 devices: a whole 2x2x4 slice. The times are simulated.
32 devices in a mesh: grp: 2 (over y), ep: 4 (over z), tp: 4 (over x, core).
Axes of the slice: x: 2, y: 2, z: 4, core: 2. Of those that a mesh axis runs over, the one named last changes fastest.
Arguments:
- queries: bfloat16 [1024, 1024], P(('grp', 'ep'), 'tp'), parts along dimension 0, may hold values from -6 to 6
- keys: bfloat16 [1024, 1024], P(('grp', 'ep'), 'tp'), parts along dimension 0, may hold values from -6 to 6
- values: bfloat16 [1024, 1024], P(('grp', 'ep'), 'tp'), parts along dimension 0, may hold values from -6 to 6
- lambdas: float32 [8], P('tp'), may hold values from 0.3 to 0.8
- head_gain: float32 [128], replicated, may hold values from 0.1 to 1.9
- tokens: bfloat16 [2048, 1536], P(('grp', 'ep')), parts along dimension 0, may hold values from -6 to 6
- route_ids: int32 [2048, 2], P(('grp', 'ep')), parts along dimension 0, may hold values from 0 to 3, all different within a row; in each aligned block of 256 rows (0 to 255, 256 to 511, ...) at most 256 rows name the same one
- route_weights: float32 [2048, 2], P(('grp', 'ep')), parts along dimension 0, may hold values from 0.2 to 1
- moe_gain: float32 [1536], replicated, may hold values from 0.1 to 1.9
- w_gate: bfloat16 [4, 1536, 3072], P('ep', None, 'tp'), may hold values from -0.15625 to 0.15625
- w_up: bfloat16 [4, 1536, 3072], P('ep', None, 'tp'), may hold values from -0.15625 to 0.15625
- w_down: bfloat16 [4, 3072, 1536], P('ep', 'tp'), may hold values from -0.109375 to 0.109375
Outputs:
- heads_out: bfloat16 [1024, 1024], P(('grp', 'ep'), 'tp'), parts along dimension 0
- expert_out: bfloat16 [2048, 1536], P(('grp', 'ep'), 'tp'), parts along dimension 0
There are 2 independent parts, one for each index of `grp`. A program takes and returns all parts, laid end to end along the dimension named above; an argument that names none is the same for every part. Nothing has to cross between parts.
Inputs may be any that keep to these rules, and one draw needn't show every extreme that they name: `route_ids`: each row names 2 different experts. In the 256 rows of one device no expert is named more than 256 times, and in every draw some device names some expert exactly 256 times.
All inputs are finite; a program needn't handle non-finite values.
Results may differ from a plain program's by a relative error of at most 0.015.
Values may be sent and summed in bfloat16 or wider, within the bound.
No kernel may reach another device: no remote copies, remote signals or barrier semaphores. Data moves between devices by JAX's collectives and lax.ppermute only.
A program may use at most 64 MiB of HBM per device.

v0:
```python
import jax
import jax.numpy as jnp
from jax import lax
from jax.sharding import PartitionSpec as P


def attend(queries, keys, values, lambdas, head_gain):
    row_count = queries.shape[0]
    head_count = lambdas.shape[0]
    head_dim = queries.shape[1] // (2 * head_count)
    value_dim = values.shape[1] // head_count
    query_parts = queries.reshape(row_count, head_count, 2, head_dim)
    score_scale = head_dim ** (-0.5)
    running = jnp.full((head_count, 2, row_count), -1e30, jnp.float32)
    key_piece = lax.all_gather(keys, "ep", axis=0, tiled=True)
    value_piece = lax.all_gather(values, "ep", axis=0, tiled=True)
    count = key_piece.shape[0]
    key_parts = key_piece.reshape(count, head_count, 2, head_dim)
    value_parts = value_piece.reshape(count, head_count, value_dim)
    scores = (
        jnp.einsum("qhcd,khcd->hcqk", query_parts, key_parts, preferred_element_type=jnp.float32)
        * score_scale
    )
    newest = jnp.maximum(running, jnp.max(scores, axis=-1))
    weights_now = jnp.exp(scores - newest[..., None])
    totals = jnp.sum(weights_now, axis=-1)
    sums = jnp.einsum(
        "hcqk,khe->hcqe",
        weights_now.astype(jnp.bfloat16),
        value_parts,
        preferred_element_type=jnp.float32,
    )
    running, totals, sums = (newest, totals, sums)
    means = sums / totals[..., None]
    mixed = means[:, 0] - lambdas[:, None, None] * means[:, 1]
    scaled = mixed * lax.rsqrt(jnp.mean(mixed * mixed, axis=-1, keepdims=True) + 1e-06) * head_gain
    return (
        jnp.transpose(scaled, (1, 0, 2))
        .reshape(row_count, head_count * value_dim)
        .astype(jnp.bfloat16)
    )


def experts(tokens, route_ids, route_weights, moe_gain, w_gate, w_up, w_down):
    row_count, width = tokens.shape
    top_count = route_ids.shape[1]
    ep_size = lax.axis_size("ep")
    tp_size = lax.axis_size("tp")
    expert_count = w_gate.shape[0] * ep_size
    capacity = 2 * row_count * top_count // expert_count
    token_float = tokens.astype(jnp.float32)
    normed = (
        token_float
        * lax.rsqrt(jnp.mean(token_float * token_float, axis=1, keepdims=True) + 1e-06)
        * moe_gain
    ).astype(jnp.bfloat16)
    flat_ids = route_ids.reshape(-1)
    onehot = (flat_ids[:, None] == jnp.arange(expert_count, dtype=jnp.int32)[None, :]).astype(
        jnp.int32
    )
    earlier = jnp.cumsum(onehot, axis=0) - onehot
    position = jnp.sum(earlier * onehot, axis=1)
    slot_index = flat_ids * capacity + position
    owners = (
        jnp.full((expert_count * capacity,), row_count, jnp.int32)
        .at[slot_index]
        .set(jnp.arange(row_count * top_count, dtype=jnp.int32) // top_count)
    )
    padded = jnp.concatenate([normed, jnp.zeros((1, width), jnp.bfloat16)], axis=0)
    outgoing = padded[owners].reshape(expert_count, capacity, width)
    gate_mat = w_gate[0]
    up_mat = w_up[0]
    down_mat = w_down[0]
    slice_width = width // tp_size
    own_columns = lax.dynamic_slice_in_dim(
        outgoing, lax.axis_index("tp") * slice_width, slice_width, 2
    )
    arrived = lax.all_to_all(own_columns, "ep", split_axis=0, concat_axis=0, tiled=True)
    piece = lax.all_gather(arrived, "tp", axis=2, tiled=True)
    gate = jnp.einsum("scd,df->scf", piece, gate_mat, preferred_element_type=jnp.float32)
    upward = jnp.einsum("scd,df->scf", piece, up_mat, preferred_element_type=jnp.float32)
    hidden = (jax.nn.silu(gate) * upward).astype(jnp.bfloat16)
    flat_hidden = hidden.reshape(-1, hidden.shape[2])
    summed = lax.psum_scatter(
        jnp.einsum("fd,sf->ds", down_mat, flat_hidden, preferred_element_type=jnp.float32).astype(
            jnp.bfloat16
        ),
        "tp",
        scatter_dimension=0,
        tiled=True,
    )
    back = lax.all_to_all(summed, "ep", split_axis=1, concat_axis=1, tiled=True)
    picked = (
        jnp.take(back, slot_index, axis=1).astype(jnp.float32).reshape(-1, row_count, top_count)
    )
    combined = jnp.einsum("drk,rk->rd", picked, route_weights)
    return combined.astype(jnp.bfloat16)


def on_device(
    queries,
    keys,
    values,
    lambdas,
    head_gain,
    tokens,
    route_ids,
    route_weights,
    moe_gain,
    w_gate,
    w_up,
    w_down,
):
    heads_out = attend(queries, keys, values, lambdas, head_gain)
    expert_out = experts(tokens, route_ids, route_weights, moe_gain, w_gate, w_up, w_down)
    return (heads_out, expert_out)


def solution(mesh):
    in_specs = (
        P(("grp", "ep"), "tp"),
        P(("grp", "ep"), "tp"),
        P(("grp", "ep"), "tp"),
        P("tp"),
        P(),
        P(("grp", "ep"), None),
        P(("grp", "ep"), None),
        P(("grp", "ep"), None),
        P(),
        P("ep", None, "tp"),
        P("ep", None, "tp"),
        P("ep", "tp", None),
    )
    out_specs = (P(("grp", "ep"), "tp"), P(("grp", "ep"), "tp"))
    return jax.shard_map(
        on_device, mesh=mesh, in_specs=in_specs, out_specs=out_specs, check_vma=False
    )
```

profile of v0, /device:TPU:0, one launch (start us, length us, event | category | flops | bytes accessed | tf_op | source)
XLA Modules:
  0.0 183.2 jit_solution(15858981580019613275)
XLA Ops:
  7.2 0.0 copy-start
  7.2 0.0 all-gather.2.cloned.1.call-start
  7.2 1.0 copy.40
  8.2 0.1 eq.26
  8.3 0.1 reshape.111
  8.5 0.7 broadcast_multiply_fusion
  9.2 1.2 reduce-window.6
  10.4 0.2 slice_reduce_fusion
  10.6 0.2 reduce-window.9
  10.8 0.1 add_bitcast_fusion
  10.9 0.1 copy.44
  11.0 0.1 mul.101
  11.2 2.4 %scatter_custom_fusion = s32[1024]{0:T(1024)S(1)} fusion(s32[512]{0:T(512)S(1)} %bitcast.95, s32[512]{0:T(512)S(1)} %add_select_fusion, s32[]{:T(128)} %constant.33.clone.1), kind=kCustom, calls=%fused_computation.53 | custom fusion | bytes 4100 | tf_op jit(solution)/shard_map/scatter | solution.py:67
  13.7 1.4 fusion.8
  15.1 1.4 fusion.10
  16.4 0.1 concatenate.3
  16.5 5.6 %gather_fusion = bf16[1024,1536]{1,0:T(8,128)(2,1)} fusion(bf16[257,1536]{1,0:T(8,128)(2,1)S(1)} %concatenate.3, s32[1024]{0:T(1024)S(1)} %fusion.23), kind=kCustom, calls=%fused_computation | custom fusion | bytes 6295552 | tf_op jit(solution)/shard_map/gather | solution.py:70
  22.1 1.2 constant_dynamic-slice_fusion
  23.3 26.4 %all_to_all.17 = bf16[4,256,384]{2,1,0:T(8,128)(2,1)} all-to-all(bf16[4,256,384]{2,1,0:T(8,128)(2,1)S(1)} %constant_dynamic-slice_fusion), channel_id=1, replica_groups=mesh['grp'=2,'ep'=4,'tp'=4] {'ep'}, dimensions={0} | all-to-all | bytes 1572864 | tf_op jit(solution)/shard_map/all_to_all | solution.py:78
  49.7 0.0 all-gather.2.cloned.1.call-update
  49.7 0.0 reduce-scatter.4.cloned.1.call-start
  49.8 27.7 %all-gather.2.cloned.1.call-done = bf16[4,256,1536]{2,1,0:T(8,128)(2,1)} async-done(((bf16[4,256,384]{2,1,0:T(8,128)(2,1)}), bf16[4,256,1536]{2,1,0:T(8,128)(2,1)}) %all-gather.2.cloned.1.call-update) | async-done | bytes 3145744 | tf_op jit(solution)/shard_map/all_gather | solution.py:79
  77.4 0.0 copy-start.8
  77.4 0.0 copy-start.9
  77.4 5.4 %fusion.2 = f32[4,256,768]{2,1,0:T(8,128)S(1)} fusion(bf16[4,256,1536]{2,1,0:T(8,128)(2,1)} %all-gather.2.cloned.1.call-done, bf16[1,1536,768]{2,1,0:T(8,128)(2,1)} %param.22), kind=kOutput, calls=%fused_computation.7 | convolution fusion | flops 2415919104 | bytes 8650752 | tf_op jit(solution)/shard_map/scd,df->scf/dot_general | solution.py:81
  82.8 0.0 copy-done.8
  82.8 0.0 copy-done.9
  82.8 2.9 %multiply_convert_fusion = bf16[4,256,768]{2,1,0:T(8,128)(2,1)S(1)} fusion(f32[4,256,768]{2,1,0:T(8,128)S(1)} %fusion.2, bf16[4,256,1536]{2,1,0:T(8,128)(2,1)S(1)} %copy-done.8, bf16[1,1536,768]{2,1,0:T(8,128)(2,1)S(1)} %copy-done.9), kind=kOutput, calls=%fused_computation.5 | convolution fusion | flops 2420637696 | bytes 10223616 | tf_op jit(solution)/shard_map/scd,df->scf/dot_general | solution.py:80
  85.7 0.0 copy-done
  85.8 4.0 %fusion = bf16[1536,1024]{0,1:T(8,128)(2,1)} fusion(bf16[1024,768]{1,0:T(8,128)(2,1)S(1)} %bitcast.99, bf16[1,768,1536]{2,1,0:T(8,128)(2,1)S(1)} %copy-done), kind=kOutput, calls=%fused_computation.4 | convolution fusion | flops 2417491968 | bytes 7077888 | tf_op jit(solution)/shard_map/fd,sf->ds/dot_general | solution.py:85
  89.8 4.6 %copy.49 = bf16[1536,1024]{1,0:T(8,128)(2,1)} copy(bf16[1536,1024]{0,1:T(8,128)(2,1)} %fusion) | data formatting | bytes 6291456
  94.4 0.0 copy-start.4
  94.4 0.0 reduce-scatter.4.cloned.1.call-update
  94.5 0.0 copy-start.2
  94.5 0.1 reduce_sum.43
  94.6 0.1 copy.42
  94.7 0.4 copy-done.4
  95.1 0.8 copy.43
  95.9 0.0 copy-done.5
  95.9 0.8 copy.47
  96.7 0.0 copy-done.1
  96.7 13.9 %all_gather.9 = bf16[512,256]{1,0:T(8,128)(2,1)S(1)} all-gather(bf16[128,256]{1,0:T(8,128)(2,1)S(1)} %copy-done.1), channel_id=1, replica_groups=mesh['grp'=2,'ep'=4,'tp'=4] {'ep'}, dimensions={0}, use_global_device_ids=true | all-gather | bytes 327680 | tf_op jit(solution)/shard_map/all_gather | solution.py:15
  110.6 0.1 copy.37
  110.8 0.0 copy-done.3
  110.8 0.1 copy.36
  110.9 1.3 fusion.30
  112.2 20.2 %reduce-scatter.4.cloned.1.call-done = bf16[384,1024]{1,0:T(8,128)(2,1)} async-done(((bf16[1536,1024]{1,0:T(8,128)(2,1)}), bf16[384,1024]{1,0:T(8,128)(2,1)}) %reduce-scatter.4.cloned.1.call-update) | async-done | bytes 786448
  132.5 2.3 %copy.50 = bf16[384,1024]{0,1:T(8,128)(2,1)} copy(bf16[384,1024]{1,0:T(8,128)(2,1)} %reduce-scatter.4.cloned.1.call-done) | data formatting | bytes 1572864
  134.8 4.7 %all-to-all-start.1 = ((bf16[384,4,256]{0,2,1:T(8,128)(2,1)}), bf16[384,4,256]{0,2,1:T(8,128)(2,1)S(1)}, u32[]{:S(2)}, u32[]{:S(2)}) async-start(bf16[384,4,256]{0,2,1:T(8,128)(2,1)} %bitcast.87), calls=%async_computation.1 | async-start | bytes 1572864 | tf_op jit(solution)/shard_map/all_to_all | solution.py:92
  139.5 0.0 copy-done.2
  139.5 27.2 %all_gather.10 = bf16[512,256]{1,0:T(8,128)(2,1)S(1)} all-gather(bf16[128,256]{1,0:T(8,128)(2,1)S(1)} %copy-done.2), channel_id=1, replica_groups=mesh['grp'=2,'ep'=4,'tp'=4] {'ep'}, dimensions={0}, use_global_device_ids=true | all-gather | bytes 327680 | tf_op jit(solution)/shard_map/all_gather | solution.py:16
  166.7 0.9 copy.38
  167.6 1.5 fusion.11
  169.1 1.7 convolution_divide_fusion
  170.9 0.0 copy-done.6
  170.9 0.1 multiply_reduce_fusion
  171.0 0.0 copy-done.7
  171.0 0.1 multiply_convert_fusion.1
  171.1 0.7 copy.45
  171.8 0.0 all-to-all-done.1
  171.8 1.9 %gather_fusion.1 = bf16[512,384]{1,0:T(8,128)(2,1)S(1)} fusion(bf16[384,1024]{0,1:T(8,128)(2,1)S(1)} %bitcast.85, s32[1024]{0:T(1024)S(1)} %pad_clamp_fusion), kind=kCustom, calls=%fused_computation.1 | custom fusion | bytes 788480 | tf_op jit(solution)/shard_map/jit(_take)/gather | solution.py:94
  173.8 0.1 gather.11
  173.9 1.7 fusion.15
  175.7 0.7 copy.55
  (15 shorter events, 0.1 us)
Async XLA Ops:
  7.2 78.6 %copy-start = (bf16[1,768,1536]{2,1,0:T(8,128)(2,1)S(1)}, bf16[1,768,1536]{2,1,0:T(8,128)(2,1)}, u32[]{:S(2)}) copy-start(bf16[1,768,1536]{2,1,0:T(8,128)(2,1)} %param.23) | copy-start | bytes 7077892
  7.2 70.3 %all-gather.2.cloned.1.call-start = ((), (), s32[]{:S(2)}) async-start(), calls=%async_computation.3 | async-start | bytes 3932160 | tf_op jit(solution)/shard_map/all_gather | solution.py:79
  49.7 82.8 %reduce-scatter.4.cloned.1.call-start = ((), (), s32[]{:S(2)}) async-start(), calls=%async_computation.4 | async-start | bytes 3932160
  77.4 5.4 %copy-start.8 = (bf16[4,256,1536]{2,1,0:T(8,128)(2,1)S(1)}, bf16[4,256,1536]{2,1,0:T(8,128)(2,1)}, u32[]{:S(2)}) copy-start(bf16[4,256,1536]{2,1,0:T(8,128)(2,1)} %all-gather.2.cloned.1.call-done) | copy-start | bytes 9437188
  77.4 5.4 %copy-start.9 = (bf16[1,1536,768]{2,1,0:T(8,128)(2,1)S(1)}, bf16[1,1536,768]{2,1,0:T(8,128)(2,1)}, u32[]{:S(2)}) copy-start(bf16[1,1536,768]{2,1,0:T(8,128)(2,1)} %param.21) | copy-start | bytes 7077892
  94.4 0.7 copy-start.4
  94.4 1.4 copy-start.5
  94.4 2.3 %copy-start.1 = (bf16[128,256]{1,0:T(8,128)(2,1)S(1)}, bf16[128,256]{1,0:T(8,128)(2,1)}, u32[]{:S(2)}) copy-start(bf16[128,256]{1,0:T(8,128)(2,1)} %param.13) | copy-start | bytes 196612
  94.4 16.4 %copy-start.3 = (bf16[128,256]{1,0:T(8,128)(2,1)S(1)}, bf16[128,256]{1,0:T(8,128)(2,1)}, u32[]{:S(2)}) copy-start(bf16[128,256]{1,0:T(8,128)(2,1)} %param.12) | copy-start | bytes 196612
  94.5 45.1 %copy-start.2 = (bf16[128,256]{1,0:T(8,128)(2,1)S(1)}, bf16[128,256]{1,0:T(8,128)(2,1)}, u32[]{:S(2)}) copy-start(bf16[128,256]{1,0:T(8,128)(2,1)} %param.14) | copy-start | bytes 196612
  112.2 58.6 %copy-start.6 = (f32[2]{0:T(128)S(1)}, f32[2]{0:T(128)}, u32[]{:S(2)}) copy-start(f32[2]{0:T(128)} %param.15) | copy-start | bytes 28
  134.8 36.2 %copy-start.7 = (f32[128]{0:T(128)S(1)}, f32[128]{0:T(128)}, u32[]{:S(2)}) copy-start(f32[128]{0:T(128)} %param.16) | copy-start | bytes 1540
  134.8 37.1 %all-to-all-start.1 = ((bf16[384,4,256]{0,2,1:T(8,128)(2,1)}), bf16[384,4,256]{0,2,1:T(8,128)(2,1)S(1)}, u32[]{:S(2)}, u32[]{:S(2)}) async-start(bf16[384,4,256]{0,2,1:T(8,128)(2,1)} %bitcast.87), calls=%async_computation.1 | async-start | bytes 1572864 | tf_op jit(solution)/shard_map/all_to_all | solution.py:92
Sparse Core Ops, SparseCore 0:
  49.8 27.5 all-gather.1
  94.6 37.8 reduce-scatter.3
where the time goes:
time: 184 us; the launch traced here: 183 us
  blocking collectives  67.5 us (37%)
  waiting for transfers between devices  48 us (26%)
  local copies, waits for them, and re-layouts  24.9 us (14%)
  matrix products  17 us (9%)
  between operations  14.3 us (8%)
  other arithmetic  6.72 us (4%)
  starting transfers between devices  4.81 us (3%)
    all_gather x1, waiting for transfers between devices, experts(): piece = lax.all_gather(arrived, 'tp', axis=2, tiled=True)  27.7 us
    all_gather x1, blocking collectives, attend(): value_piece = lax.all_gather(values, 'ep', axis=0, tiled=True)  27.2 us
    all_to_all x1, blocking collectives, experts(): lax.all_to_all(own_columns, 'ep', split_axis=0, concat_axis=0, tiled=True)  26.4 us
    unnamed x3, waiting for transfers between devices  20.3 us
    all_gather x1, blocking collectives, attend(): key_piece = lax.all_gather(keys, 'ep', axis=0, tiled=True)  13.9 us
    unnamed x26, local copies, waits for them, and re-layouts  10 us
    gather x1, local copies, waits for them, and re-layouts, experts(): outgoing = padded[owners].reshape(expert_count, capacity, width)  5.61 us
    dot_general x1, matrix products, experts(): jnp.einsum('scd,df->scf', piece, up_mat, preferred_element_type=jnp.float32)  5.36 us
  transfers between devices with their start and end apart: 3, of which 2 were waited for; matrix products, arithmetic and copies ran while one was open for 5% of the time, Pallas kernels for 0%

commit v1 on v0

--- a/solution.py
+++ b/solution.py
@@ -2,6 +2,31 @@
 import jax.numpy as jnp
 from jax import lax
 from jax.sharding import PartitionSpec as P
+
+
+def xor_pairs(size, step):
+    return [(i, i ^ step) for i in range(size)]
+
+
+def halving_steps(size):
+    steps = []
+    step = size // 2
+    while step >= 1:
+        steps.append(step)
+        step //= 2
+    return steps
+
+
+def power_of_two(size):
+    return size & (size - 1) == 0
+
+
+def gathered(piece):
+    size = lax.axis_size("ep")
+    pieces = [piece]
+    for step in range(1, size):
+        pieces.append(lax.ppermute(piece, "ep", xor_pairs(size, step)))
+    return jnp.concatenate(pieces, axis=0)
 
 
 def attend(queries, keys, values, lambdas, head_gain):
@@ -11,9 +36,12 @@
     value_dim = values.shape[1] // head_count
     query_parts = queries.reshape(row_count, head_count, 2, head_dim)
     score_scale = head_dim ** (-0.5)
-    running = jnp.full((head_count, 2, row_count), -1e30, jnp.float32)
-    key_piece = lax.all_gather(keys, "ep", axis=0, tiled=True)
-    value_piece = lax.all_gather(values, "ep", axis=0, tiled=True)
+    if power_of_two(lax.axis_size("ep")) and lax.axis_size("ep") <= 4:
+        both = gathered(jnp.concatenate([keys, values], axis=1))
+        key_piece, value_piece = both[:, : keys.shape[1]], both[:, keys.shape[1] :]
+    else:
+        key_piece = lax.all_gather(keys, "ep", axis=0, tiled=True)
+        value_piece = lax.all_gather(values, "ep", axis=0, tiled=True)
     count = key_piece.shape[0]
     key_parts = key_piece.reshape(count, head_count, 2, head_dim)
     value_parts = value_piece.reshape(count, head_count, value_dim)
@@ -21,7 +49,7 @@
         jnp.einsum("qhcd,khcd->hcqk", query_parts, key_parts, preferred_element_type=jnp.float32)
         * score_scale
     )
-    newest = jnp.maximum(running, jnp.max(scores, axis=-1))
+    newest = jnp.max(scores, axis=-1)
     weights_now = jnp.exp(scores - newest[..., None])
     totals = jnp.sum(weights_now, axis=-1)
     sums = jnp.einsum(
@@ -30,7 +58,6 @@
         value_parts,
         preferred_element_type=jnp.float32,
     )
-    running, totals, sums = (newest, totals, sums)
     means = sums / totals[..., None]
     mixed = means[:, 0] - lambdas[:, None, None] * means[:, 1]
     scaled = mixed * lax.rsqrt(jnp.mean(mixed * mixed, axis=-1, keepdims=True) + 1e-06) * head_gain
@@ -41,19 +68,91 @@
     )
 
 
-def experts(tokens, route_ids, route_weights, moe_gain, w_gate, w_up, w_down):
+def normalize(tokens, moe_gain):
+    token_float = tokens.astype(jnp.float32)
+    return (
+        token_float
+        * lax.rsqrt(jnp.mean(token_float * token_float, axis=1, keepdims=True) + 1e-06)
+        * moe_gain
+    ).astype(jnp.bfloat16)
+
+
+def experts_whole(tokens, route_ids, route_weights, moe_gain, w_gate, w_up, w_down):
+    row_count, width = tokens.shape
+    ep_size = lax.axis_size("ep")
+    tp_size = lax.axis_size("tp")
+    ep_index = lax.axis_index("ep")
+    tp_index = lax.axis_index("tp")
+    steps = halving_steps(tp_size)
+    piece_rows = row_count // tp_size
+    part = jnp.zeros((), jnp.int32)
+    for place, step in enumerate(steps):
+        part = part + jnp.where(tp_index & step != 0, 1 << place, 0)
+    mine = normalize(
+        lax.dynamic_slice_in_dim(tokens, part * piece_rows, piece_rows, 0), moe_gain
+    )
+    arrivals = [
+        lax.ppermute(mine, "ep", xor_pairs(ep_size, step)) for step in range(1, ep_size)
+    ]
+    gate_mat, up_mat = w_gate[0], w_up[0]
+    slice_width = width // tp_size
+    order = []
+    for place in range(tp_size):
+        target = tp_index
+        for bit, step in enumerate(steps):
+            if not (place >> bit) & 1:
+                target = target ^ step
+        order.append(target)
+    down_mat = jnp.concatenate(
+        [lax.dynamic_slice_in_dim(w_down[0], t * slice_width, slice_width, 1) for t in order],
+        axis=1,
+    )
+
+    def all_rows(piece):
+        for step in steps:
+            other = lax.ppermute(piece, "tp", xor_pairs(tp_size, step))
+            low = tp_index & step == 0
+            piece = jnp.concatenate(
+                [jnp.where(low, piece, other), jnp.where(low, other, piece)], axis=0
+            )
+        return piece
+
+    def expert(rows):
+        gate = jnp.dot(rows, gate_mat, preferred_element_type=jnp.float32)
+        upward = jnp.dot(rows, up_mat, preferred_element_type=jnp.float32)
+        hidden = (jax.nn.silu(gate) * upward).astype(jnp.bfloat16)
+        partial = jnp.dot(hidden, down_mat, preferred_element_type=jnp.float32).astype(
+            jnp.bfloat16
+        )
+        for step in reversed(steps):
+            half = partial.shape[1] // 2
+            other = lax.ppermute(partial[:, :half], "tp", xor_pairs(tp_size, step))
+            partial = (
+                partial[:, half:].astype(jnp.float32) + other.astype(jnp.float32)
+            ).astype(jnp.bfloat16)
+        return partial
+
+    results = [expert(normalize(tokens, moe_gain))]
+    for step in range(1, ep_size):
+        done = expert(all_rows(arrivals[step - 1]))
+        results.append(lax.ppermute(done, "ep", xor_pairs(ep_size, step)))
+    total = jnp.zeros((row_count, slice_width), jnp.float32)
+    for step in range(ep_size):
+        named = route_ids == (ep_index ^ step)
+        weight = jnp.sum(jnp.where(named, route_weights, 0.0), axis=1, keepdims=True)
+        here = jnp.any(named, axis=1, keepdims=True)
+        total = total + jnp.where(here, results[step].astype(jnp.float32) * weight, 0.0)
+    return total.astype(jnp.bfloat16)
+
+
+def experts_slots(tokens, route_ids, route_weights, moe_gain, w_gate, w_up, w_down):
     row_count, width = tokens.shape
     top_count = route_ids.shape[1]
     ep_size = lax.axis_size("ep")
     tp_size = lax.axis_size("tp")
     expert_count = w_gate.shape[0] * ep_size
     capacity = 2 * row_count * top_count // expert_count
-    token_float = tokens.astype(jnp.float32)
-    normed = (
-        token_float
-        * lax.rsqrt(jnp.mean(token_float * token_float, axis=1, keepdims=True) + 1e-06)
-        * moe_gain
-    ).astype(jnp.bfloat16)
+    normed = normalize(tokens, moe_gain)
     flat_ids = route_ids.reshape(-1)
     onehot = (flat_ids[:, None] == jnp.arange(expert_count, dtype=jnp.int32)[None, :]).astype(
         jnp.int32
@@ -95,6 +194,23 @@
     )
     combined = jnp.einsum("drk,rk->rd", picked, route_weights)
     return combined.astype(jnp.bfloat16)
+
+
+def experts(tokens, route_ids, route_weights, moe_gain, w_gate, w_up, w_down):
+    row_count = tokens.shape[0]
+    ep_size = lax.axis_size("ep")
+    tp_size = lax.axis_size("tp")
+    expert_count = w_gate.shape[0] * ep_size
+    capacity = 2 * row_count * route_ids.shape[1] // expert_count
+    whole = (
+        capacity >= row_count
+        and w_gate.shape[0] == 1
+        and power_of_two(ep_size)
+        and power_of_two(tp_size)
+        and row_count % tp_size == 0
+    )
+    chosen = experts_whole if whole else experts_slots
+    return chosen(tokens, route_ids, route_weights, moe_gain, w_gate, w_up, w_down)
 
 
 def on_device(

time: 184 us -> 116 us (0.63)
  blocking collectives: 67.5 us -> 0 us
  waiting for transfers between devices: 48 us -> 22.2 us
  starting transfers between devices: 4.81 us -> 27 us
  other arithmetic: 6.72 us -> 21.2 us
  between operations: 14.3 us -> 1.05 us
  matrix products: 17 us -> 28.2 us
  local copies, waits for them, and re-layouts: 24.9 us -> 15.6 us
    all_gather x2 -> x0, blocking collectives: 41.2 us -> none  [the longest x1 27.2 us: attend(): value_piece = lax.all_gather(values, 'ep', axis=0, tiled=True)]
    all_gather x1 -> x0, waiting for transfers between devices: 27.7 us -> none  [experts(): piece = lax.all_gather(arrived, 'tp', axis=2, tiled=True)]
    ppermute x0 -> x23, starting transfers between devices: none -> 27 us  [the longest x3 7.04 us: experts_whole(): results.append(lax.ppermute(done, 'ep', xor_pairs(ep_size, step)))]
    all_to_all x1 -> x0, blocking collectives: 26.4 us -> none  [experts(): lax.all_to_all(own_columns, 'ep', split_axis=0, concat_axis=0, tiled=True)]
    ppermute x0 -> x23, waiting for transfers between devices: none -> 22.2 us  [the longest x3 9.15 us: experts_whole(): results.append(lax.ppermute(done, 'ep', xor_pairs(ep_size, step)))]
    unnamed x3 -> x0, waiting for transfers between devices: 20.3 us -> none
    dot_general x4 -> x8, matrix products: 14 us -> 27.5 us  [the longest x4 18.7 us: expert(): jnp.dot(hidden, down_mat, preferred_element_type=jnp.float32)]
    gather x3 -> x0, local copies, waits for them, and re-layouts: 7.7 us -> none  [the longest x1 5.61 us: experts(): outgoing = padded[owners].reshape(expert_count, capacity, width)]
  transfers between devices with their start and end apart: 3 -> 23, of which waited for: 2 -> 8; matrix products, arithmetic and copies ran while one was open for 5% -> 51% of each run, Pallas kernels for 0% -> 0%
where the time goes in v1:
time: 116 us; the launch traced here: 115 us
  matrix products  28.2 us (24%)
  starting transfers between devices  27 us (23%)
  waiting for transfers between devices  22.2 us (19%)
  other arithmetic  21.2 us (18%)
  local copies, waits for them, and re-layouts  15.6 us (13%)
    dot_general x4, matrix products, expert(): jnp.dot(hidden, down_mat, preferred_element_type=jnp.float32)  18.7 us
    ppermute x3, waiting for transfers between devices, experts_whole(): results.append(lax.ppermute(done, 'ep', xor_pairs(ep_size, step)))  9.15 us
    dot_general x4, matrix products, expert(): gate = jnp.dot(rows, gate_mat, preferred_element_type=jnp.float32)  8.85 us
    slice x8, local copies, waits for them, and re-layouts, expert(): other = lax.ppermute(partial[:, :half], 'tp', xor_pairs(tp_size, step))  7.56 us
    ppermute x3, starting transfers between devices, experts_whole(): results.append(lax.ppermute(done, 'ep', xor_pairs(ep_size, step)))  7.04 us
    ppermute x3, starting transfers between devices, gathered(): pieces.append(lax.ppermute(piece, 'ep', xor_pairs(size, step)))  5.64 us
    convert_element_type x7, other arithmetic, expert(): partial = (partial[:, half:].astype(jnp.float32) + other.astype(jnp.float...  5.56 us
    ppermute x6, waiting for transfers between devices, all_rows(): other = lax.ppermute(piece, 'tp', xor_pairs(tp_size, step))  5.44 us
  transfers between devices with their start and end apart: 23, of which 8 were waited for; matrix products, arithmetic and copies ran while one was open for 51% of the time, Pallas kernels for 0%

profile of v1, /device:TPU:0, one launch (start us, length us, event | category | flops | bytes accessed | tf_op | source)
XLA Modules:
  0.0 115.2 jit_solution(10636690389110641818)
XLA Ops:
  0.6 1.0 constant_dynamic-update-slice_fusion.1
  1.6 0.8 constant_dynamic-update-slice_fusion
  2.5 5.1 %collective-permute-start.2 = (bf16[128,512]{1,0:T(8,128)(2,1)S(1)}, bf16[128,512]{1,0:T(8,128)(2,1)}, u32[]{:S(2)}, u32[]{:S(2)}) collective-permute-start(bf16[128,512]{1,0:T(8,128)(2,1)S(1)} %constant_dynamic-update-slice_fusion), channel_id=1, source_target_pairs={{0,12},{4,8},{8,4},{12,0},{1,13},{5,9},{9,5},{13,1},{2,14},{6,10},... | collective-permute-start | bytes 393224 | tf_op jit(solution)/shard_map/ppermute | solution.py:28
  7.6 0.6 collective-permute-start
  8.1 1.1 fusion.49
  9.2 1.1 fusion.51
  10.3 3.9 %collective-permute-start.17 = (bf16[64,1536]{1,0:T(8,128)(2,1)S(1)}, bf16[64,1536]{1,0:T(8,128)(2,1)}, u32[]{:S(2)}, u32[]{:S(2)}) collective-permute-start(bf16[64,1536]{1,0:T(8,128)(2,1)S(1)} %fusion.51), channel_id=1, source_target_pairs={{0,12},{4,8},{8,4},{12,0},{1,13},{5,9},{9,5},{13,1},{2,14},{6,10},... | collective-permute-start | bytes 589832 | tf_op jit(solution)/shard_map/ppermute | solution.py:95
  14.2 1.4 %fusion.16 = f32[256]{0:T(256)S(1)} fusion(bf16[256,1536]{1,0:T(8,128)(2,1)} %param.17), kind=kLoop, calls=%fused_computation.23 | loop fusion | flops 1179392 | bytes 787456 | tf_op jit(solution)/shard_map/reduce_sum | solution.py:75
  15.6 3.8 %fusion.14 = f32[256,768]{1,0:T(8,128)} fusion(bf16[1,1536,768]{2,1,0:T(8,128)(2,1)} %param.21, bf16[256,1536]{1,0:T(8,128)(2,1)} %param.17, f32[1536]{0:T(1024)} %param.20, f32[256]{0:T(256)S(1)} %add_rsqrt_fusion), kind=kOutput, calls=%fused_computation.19 | convolution fusion | flops 605552640 | bytes 3939328 | tf_op jit(solution)/shard_map/dot_general | solution.py:121
  19.4 1.5 %dynamic-slice_bitcast_fusion.3 = (bf16[768,384]{1,0:T(8,128)(2,1)}, bf16[768,384]{1,0:T(8,128)(2,1)}, bf16[768,384]{1,0:T(8,128)(2,1)}, bf16[768,384]{1,0:T(8,128)(2,1)}) fusion(bf16[1,768,1536]{2,1,0:T(8,128)(2,1)S(1)} %copy-done.1, s32[]{:T(128)S(6)} %select_n.104, s32[]{:T(128)S(6)} %select_n.105, s32[]{:T(128)S(6)} %select_n.107, s32[]{:T(128)S(6)} %select_n.106), kind=kLoop, calls=%fused_computation.52 | loop fusion | bytes 4718608 | tf_op jit(solution)/shard_map/dynamic_slice | solution.py:107
  20.9 4.5 %convolution_convert_fusion.3 = bf16[256,1536]{1,0:T(8,128)(2,1)} fusion(bf16[1,1536,768]{2,1,0:T(8,128)(2,1)S(1)} %copy-done, f32[256,768]{1,0:T(8,128)} %fusion.14, bf16[256,1536]{1,0:T(8,128)(2,1)S(1)} %copy-done.2, f32[1536]{0:T(1024)S(1)} %copy-done.15, f32[256]{0:T(256)S(1)} %add_rsqrt_fusion, bf16[768,384]{1,0:T(8,128)(2,1)} %get-tuple-element.16, ...), kind=kOutput, calls=%fused_computation.3 | convolution fusion | flops 1220542464 | bytes 7085056 | tf_op jit(solution)/shard_map/dot_general | solution.py:124
  25.4 0.6 fusion.74
  26.0 0.9 copy.21
  27.0 1.8 %slice.85 = bf16[256,768]{1,0:T(8,128)(2,1)} slice(bf16[256,1536]{1,0:T(8,128)(2,1)} %convolution_convert_fusion.3), slice={[0:256], [0:768]} | slice | bytes 786432 | tf_op jit(solution)/shard_map/slice | solution.py:129
  28.8 1.3 %select_reduce_fusion.3 = (f32[256]{0:T(256)S(1)}, f32[256]{0:T(256)S(1)}, f32[256]{0:T(256)S(1)}, f32[256]{0:T(256)}) fusion(f32[256,2]{0,1:T(2,128)} %param.19, s32[256,2]{0,1:T(2,128)S(1)} %copy-done.16, s32[]{:T(128)S(6)} %axis_index.23, s32[]{:T(128)S(6)} %xor.22, s32[]{:T(128)S(6)} %xor.24, s32[]{:T(128)S(6)} %xor.23), kind=kLoop, calls=%fused_computation.95 | loop fusion | flops 5120 | bytes 8208 | tf_op jit(solution)/shard_map/reduce_sum | solution.py:142
  30.1 0.6 collective-permute-start.5
  30.7 1.1 pad_maximum_fusion.4
  32.1 0.4 fusion.79
  32.7 0.3 convolution_divide_fusion
  33.1 1.7 %collective-permute-start.18 = (bf16[64,1536]{1,0:T(8,128)(2,1)}, bf16[64,1536]{1,0:T(8,128)(2,1)S(1)}, u32[]{:S(2)}, u32[]{:S(2)}) collective-permute-start(bf16[64,1536]{1,0:T(8,128)(2,1)} %collective-permute-done.17), channel_id=1, source_target_pairs={{0,2},{1,3},{2,0},{3,1},{4,6},{5,7},{6,4},{7,5},{8,10},{9,11},{10,... | collective-permute-start | bytes 589832 | tf_op jit(solution)/shard_map/ppermute | solution.py:113
  34.8 0.9 collective-permute-done.11
  35.7 1.5 %collective-permute-start.12 = (bf16[64,1536]{1,0:T(8,128)(2,1)}, bf16[64,1536]{1,0:T(8,128)(2,1)S(1)}, u32[]{:S(2)}, u32[]{:S(2)}) collective-permute-start(bf16[64,1536]{1,0:T(8,128)(2,1)} %collective-permute-done.11), channel_id=1, source_target_pairs={{0,2},{1,3},{2,0},{3,1},{4,6},{5,7},{6,4},{7,5},{8,10},{9,11},{10,... | collective-permute-start | bytes 589832 | tf_op jit(solution)/shard_map/ppermute | solution.py:113
  37.2 2.2 %collective-permute-done.5 = bf16[64,1536]{1,0:T(8,128)(2,1)} collective-permute-done((bf16[64,1536]{1,0:T(8,128)(2,1)S(1)}, bf16[64,1536]{1,0:T(8,128)(2,1)}, u32[]{:S(2)}, u32[]{:S(2)}) %collective-permute-start.5) | collective-permute-done | bytes 196640 | tf_op jit(solution)/shard_map/ppermute | solution.py:95
  39.4 1.5 %collective-permute-start.6 = (bf16[64,1536]{1,0:T(8,128)(2,1)}, bf16[64,1536]{1,0:T(8,128)(2,1)S(1)}, u32[]{:S(2)}, u32[]{:S(2)}) collective-permute-start(bf16[64,1536]{1,0:T(8,128)(2,1)} %collective-permute-done.5), channel_id=1, source_target_pairs={{0,2},{1,3},{2,0},{3,1},{4,6},{5,7},{6,4},{7,5},{8,10},{9,11},{10,... | collective-permute-start | bytes 589832 | tf_op jit(solution)/shard_map/ppermute | solution.py:113
  41.2 1.0 broadcast_select_fusion.7
  42.3 3.1 %collective-permute-done.12 = bf16[64,1536]{1,0:T(8,128)(2,1)S(1)} collective-permute-done((bf16[64,1536]{1,0:T(8,128)(2,1)}, bf16[64,1536]{1,0:T(8,128)(2,1)S(1)}, u32[]{:S(2)}, u32[]{:S(2)}) %collective-permute-start.12) | collective-permute-done | bytes 196640 | tf_op jit(solution)/shard_map/ppermute | solution.py:113
  45.4 1.0 broadcast_select_fusion.9
  46.4 0.8 pad_maximum_fusion.24
  47.2 2.0 %collective-permute-done.6 = bf16[64,1536]{1,0:T(8,128)(2,1)S(1)} collective-permute-done((bf16[64,1536]{1,0:T(8,128)(2,1)}, bf16[64,1536]{1,0:T(8,128)(2,1)S(1)}, u32[]{:S(2)}, u32[]{:S(2)}) %collective-permute-start.6) | collective-permute-done | bytes 196640 | tf_op jit(solution)/shard_map/ppermute | solution.py:113
  49.1 1.0 broadcast_select_fusion.11
  50.1 0.8 pad_maximum_fusion.23
  50.9 1.1 add_convert_fusion.3
  52.0 0.7 slice.87
  52.7 1.6 %collective-permute-start.4 = (bf16[256,384]{1,0:T(8,128)(2,1)}, bf16[256,384]{1,0:T(8,128)(2,1)}, u32[]{:S(2)}, u32[]{:S(2)}) collective-permute-start(bf16[256,384]{1,0:T(8,128)(2,1)} %slice.87), channel_id=1, source_target_pairs={{0,2},{1,3},{2,0},{3,1},{4,6},{5,7},{6,4},{7,5},{8,10},{9,11},{10,... | collective-permute-start | bytes 589832 | tf_op jit(solution)/shard_map/ppermute | solution.py:129
  54.5 0.8 copy-done.11
  55.4 1.7 %fusion.8 = f32[256,768]{1,0:T(8,128)} fusion(bf16[1,1536,768]{2,1,0:T(8,128)(2,1)S(1)} %copy-done.25, bf16[128,1536]{1,0:T(8,128)(2,1)S(1)} %get-tuple-element.23, bf16[128,1536]{1,0:T(8,128)(2,1)S(1)} %get-tuple-element.22), kind=kOutput, calls=%fused_computation.13 | convolution fusion | flops 605552640 | bytes 3932160 | tf_op jit(solution)/shard_map/dot_general | solution.py:121
  57.1 4.7 %convolution_convert_fusion = bf16[256,1536]{1,0:T(8,128)(2,1)} fusion(f32[256,768]{1,0:T(8,128)} %fusion.8, bf16[1,1536,768]{2,1,0:T(8,128)(2,1)S(1)} %copy-done, bf16[128,1536]{1,0:T(8,128)(2,1)} %copy-done.12, bf16[128,1536]{1,0:T(8,128)(2,1)} %copy-done.11, bf16[768,384]{1,0:T(8,128)(2,1)} %get-tuple-element.16, bf16[768,384]{1,0:T(8,128)(2,1)} %get-tuple-element.17, ...), kind=kOutput, calls=%fused_computation | convolution fusion | flops 1220542464 | bytes 7077888 | tf_op jit(solution)/shard_map/dot_general | solution.py:124
  61.8 1.9 %slice.97 = bf16[256,768]{1,0:T(8,128)(2,1)} slice(bf16[256,1536]{1,0:T(8,128)(2,1)} %convolution_convert_fusion), slice={[0:256], [0:768]} | slice | bytes 786432 | tf_op jit(solution)/shard_map/slice | solution.py:129
  63.9 1.1 broadcast_select_fusion.3
  65.1 0.7 copy-done.13
  66.0 1.7 %fusion.10 = f32[256,768]{1,0:T(8,128)} fusion(bf16[1,1536,768]{2,1,0:T(8,128)(2,1)S(1)} %copy-done.26, bf16[128,1536]{1,0:T(8,128)(2,1)S(1)} %get-tuple-element.21, bf16[128,1536]{1,0:T(8,128)(2,1)S(1)} %get-tuple-element.20), kind=kOutput, calls=%fused_computation.15 | convolution fusion | flops 605552640 | bytes 3932160 | tf_op jit(solution)/shard_map/dot_general | solution.py:121
  67.6 4.7 %convolution_convert_fusion.1 = bf16[256,1536]{1,0:T(8,128)(2,1)} fusion(f32[256,768]{1,0:T(8,128)} %fusion.10, bf16[1,1536,768]{2,1,0:T(8,128)(2,1)S(1)} %copy-done, bf16[128,1536]{1,0:T(8,128)(2,1)} %copy-done.14, bf16[128,1536]{1,0:T(8,128)(2,1)} %copy-done.13, bf16[768,384]{1,0:T(8,128)(2,1)} %get-tuple-element.16, ...), kind=kOutput, calls=%fused_computation.1 | convolution fusion | flops 1220542464 | bytes 7077888 | tf_op jit(solution)/shard_map/dot_general | solution.py:124
  72.4 1.9 %slice.93 = bf16[256,768]{1,0:T(8,128)(2,1)} slice(bf16[256,1536]{1,0:T(8,128)(2,1)} %convolution_convert_fusion.1), slice={[0:256], [0:768]} | slice | bytes 786432 | tf_op jit(solution)/shard_map/slice | solution.py:129
  74.6 1.1 broadcast_select_fusion.5
  75.7 0.7 copy-done.9
  76.6 1.7 %fusion.12 = f32[256,768]{1,0:T(8,128)} fusion(bf16[1,1536,768]{2,1,0:T(8,128)(2,1)S(1)} %copy-done.27, bf16[128,1536]{1,0:T(8,128)(2,1)S(1)} %get-tuple-element.19, bf16[128,1536]{1,0:T(8,128)(2,1)S(1)} %get-tuple-element.18), kind=kOutput, calls=%fused_computation.17 | convolution fusion | flops 605552640 | bytes 3932160 | tf_op jit(solution)/shard_map/dot_general | solution.py:121
  78.2 4.8 %convolution_convert_fusion.2 = bf16[256,1536]{1,0:T(8,128)(2,1)} fusion(f32[256,768]{1,0:T(8,128)} %fusion.12, bf16[1,1536,768]{2,1,0:T(8,128)(2,1)S(1)} %copy-done, bf16[128,1536]{1,0:T(8,128)(2,1)} %copy-done.10, bf16[128,1536]{1,0:T(8,128)(2,1)} %copy-done.9, bf16[768,384]{1,0:T(8,128)(2,1)} %get-tuple-element.16, ...), kind=kOutput, calls=%fused_computation.2 | convolution fusion | flops 1220542464 | bytes 7077888 | tf_op jit(solution)/shard_map/dot_general | solution.py:124
  83.0 1.1 slice.89
  84.4 1.1 add_convert_fusion
  85.6 0.5 collective-permute-start.21
  86.1 1.1 add_convert_fusion.1
  87.2 1.7 %collective-permute-start.15 = (bf16[256,384]{1,0:T(8,128)(2,1)S(1)}, bf16[256,384]{1,0:T(8,128)(2,1)S(1)}, u32[]{:S(2)}, u32[]{:S(2)}) collective-permute-start(bf16[256,384]{1,0:T(8,128)(2,1)S(1)} %slice.95), channel_id=1, source_target_pairs={{0,2},{1,3},{2,0},{3,1},{4,6},{5,7},{6,4},{7,5},{8,10},{9,11},{10,... | collective-permute-start | bytes 589832 | tf_op jit(solution)/shard_map/ppermute | solution.py:129
  89.1 0.5 collective-permute-start.9
  89.5 3.9 %collective-permute-done.21 = bf16[256,384]{1,0:T(8,128)(2,1)S(1)} collective-permute-done((bf16[256,384]{1,0:T(8,128)(2,1)S(1)}, bf16[256,384]{1,0:T(8,128)(2,1)S(1)}, u32[]{:S(2)}, u32[]{:S(2)}) %collective-permute-start.21) | collective-permute-done | bytes 196640 | tf_op jit(solution)/shard_map/ppermute | solution.py:129
  93.4 0.7 add_convert_fusion.5
  94.2 3.6 %collective-permute-start.22 = (bf16[256,384]{1,0:T(8,128)(2,1)}, bf16[256,384]{1,0:T(8,128)(2,1)S(1)}, u32[]{:S(2)}, u32[]{:S(2)}) collective-permute-start(bf16[256,384]{1,0:T(8,128)(2,1)} %add_convert_fusion.5), channel_id=1, source_target_pairs={{0,12},{4,8},{8,4},{12,0},{1,13},{5,9},{9,5},{13,1},{2,14},{6,10},... | collective-permute-start | bytes 589832 | tf_op jit(solution)/shard_map/ppermute | solution.py:138
  97.8 0.7 add_convert_fusion.6
  98.5 2.1 %collective-permute-start.16 = (bf16[256,384]{1,0:T(8,128)(2,1)}, bf16[256,384]{1,0:T(8,128)(2,1)S(1)}, u32[]{:S(2)}, u32[]{:S(2)}) collective-permute-start(bf16[256,384]{1,0:T(8,128)(2,1)} %add_convert_fusion.6), channel_id=1, source_target_pairs={{0,8},{4,12},{8,0},{12,4},{1,9},{5,13},{9,1},{13,5},{2,10},{6,14},... | collective-permute-start | bytes 589832 | tf_op jit(solution)/shard_map/ppermute | solution.py:138
  100.6 0.6 collective-permute-done.9
  101.2 0.7 add_convert_fusion.7
  101.9 1.3 %collective-permute-start.10 = (bf16[256,384]{1,0:T(8,128)(2,1)}, bf16[256,384]{1,0:T(8,128)(2,1)S(1)}, u32[]{:S(2)}, u32[]{:S(2)}) collective-permute-start(bf16[256,384]{1,0:T(8,128)(2,1)} %add_convert_fusion.7), channel_id=1, source_target_pairs={{0,4},{4,0},{8,12},{12,8},{1,5},{5,1},{9,13},{13,9},{2,6},{6,2},{1... | collective-permute-start | bytes 589832 | tf_op jit(solution)/shard_map/ppermute | solution.py:138
  103.4 0.7 copy.25
  104.1 9.1 %collective-permute-done.16 = bf16[256,384]{1,0:T(8,128)(2,1)S(1)} collective-permute-done((bf16[256,384]{1,0:T(8,128)(2,1)}, bf16[256,384]{1,0:T(8,128)(2,1)S(1)}, u32[]{:S(2)}, u32[]{:S(2)}) %collective-permute-start.16) | collective-permute-done | bytes 196640 | tf_op jit(solution)/shard_map/ppermute | solution.py:138
  113.3 1.9 %add_convert_fusion.4 = bf16[256,384]{1,0:T(8,128)(2,1)} fusion(bf16[256,384]{1,0:T(8,128)(2,1)S(1)} %collective-permute-done.22, bf16[256,384]{1,0:T(8,128)(2,1)S(1)} %collective-permute-done.16, bf16[256,384]{1,0:T(8,128)(2,1)S(1)} %collective-permute-done.10, bf16[256,384]{1,0:T(8,128)(2,1)} %collective-permute-done.4, ...), kind=kLoop, calls=%fused_computation.63 | loop fusion | flops 1966080 | bytes 1184768 | tf_op jit(solution)/shard_map/convert_element_type | solution.py:145
  (93 shorter events, 2.8 us)
Async XLA Ops:
  0.6 20.3 %copy-start = (bf16[1,1536,768]{2,1,0:T(8,128)(2,1)S(1)}, bf16[1,1536,768]{2,1,0:T(8,128)(2,1)}, u32[]{:S(2)}) copy-start(bf16[1,1536,768]{2,1,0:T(8,128)(2,1)} %param.22) | copy-start | bytes 7077892
  2.5 27.6 %collective-permute-start.2 = (bf16[128,512]{1,0:T(8,128)(2,1)S(1)}, bf16[128,512]{1,0:T(8,128)(2,1)}, u32[]{:S(2)}, u32[]{:S(2)}) collective-permute-start(bf16[128,512]{1,0:T(8,128)(2,1)S(1)} %constant_dynamic-update-slice_fusion), channel_id=1, source_target_pairs={{0,12},{4,8},{8,4},{12,0},{1,13},{5,9},{9,5},{13,1},{2,14},{6,10},... | collective-permute-start | bytes 393224 | tf_op jit(solution)/shard_map/ppermute | solution.py:28
  7.6 23.1 %collective-permute-start.1 = (bf16[128,512]{1,0:T(8,128)(2,1)S(1)}, bf16[128,512]{1,0:T(8,128)(2,1)}, u32[]{:S(2)}, u32[]{:S(2)}) collective-permute-start(bf16[128,512]{1,0:T(8,128)(2,1)S(1)} %constant_dynamic-update-slice_fusion), channel_id=1, source_target_pairs={{0,8},{4,12},{8,0},{12,4},{1,9},{5,13},{9,1},{13,5},{2,10},{6,14},... | collective-permute-start | bytes 393224 | tf_op jit(solution)/shard_map/ppermute | solution.py:28
  7.6 23.1 %collective-permute-start = (bf16[128,512]{1,0:T(8,128)(2,1)S(1)}, bf16[128,512]{1,0:T(8,128)(2,1)}, u32[]{:S(2)}, u32[]{:S(2)}) collective-permute-start(bf16[128,512]{1,0:T(8,128)(2,1)S(1)} %constant_dynamic-update-slice_fusion), channel_id=1, source_target_pairs={{0,4},{4,0},{8,12},{12,8},{1,5},{5,1},{9,13},{13,9},{2,6},{6,2},{1... | collective-permute-start | bytes 393224 | tf_op jit(solution)/shard_map/ppermute | solution.py:28
  10.3 22.9 %collective-permute-start.17 = (bf16[64,1536]{1,0:T(8,128)(2,1)S(1)}, bf16[64,1536]{1,0:T(8,128)(2,1)}, u32[]{:S(2)}, u32[]{:S(2)}) collective-permute-start(bf16[64,1536]{1,0:T(8,128)(2,1)S(1)} %fusion.51), channel_id=1, source_target_pairs={{0,12},{4,8},{8,4},{12,0},{1,13},{5,9},{9,5},{13,1},{2,14},{6,10},... | collective-permute-start | bytes 589832 | tf_op jit(solution)/shard_map/ppermute | solution.py:95
  14.2 21.5 %collective-permute-start.11 = (bf16[64,1536]{1,0:T(8,128)(2,1)S(1)}, bf16[64,1536]{1,0:T(8,128)(2,1)}, u32[]{:S(2)}, u32[]{:S(2)}) collective-permute-start(bf16[64,1536]{1,0:T(8,128)(2,1)S(1)} %fusion.51), channel_id=1, source_target_pairs={{0,8},{4,12},{8,0},{12,4},{1,9},{5,13},{9,1},{13,5},{2,10},{6,14},... | collective-permute-start | bytes 589832 | tf_op jit(solution)/shard_map/ppermute | solution.py:95
  15.6 3.8 %copy-start.1 = (bf16[1,768,1536]{2,1,0:T(8,128)(2,1)S(1)}, bf16[1,768,1536]{2,1,0:T(8,128)(2,1)}, u32[]{:S(2)}) copy-start(bf16[1,768,1536]{2,1,0:T(8,128)(2,1)} %param.23) | copy-start | bytes 7077892
  19.4 1.5 %copy-start.2 = (bf16[256,1536]{1,0:T(8,128)(2,1)S(1)}, bf16[256,1536]{1,0:T(8,128)(2,1)}, u32[]{:S(2)}) copy-start(bf16[256,1536]{1,0:T(8,128)(2,1)} %param.17) | copy-start | bytes 2359300
  19.4 1.5 %copy-start.15 = (f32[1536]{0:T(1024)S(1)}, f32[1536]{0:T(1024)}, u32[]{:S(2)}) copy-start(f32[1536]{0:T(1024)} %param.20) | copy-start | bytes 18436
  20.9 4.5 %copy-start.16 = (s32[256,2]{0,1:T(2,128)S(1)}, s32[256,2]{0,1:T(2,128)}, u32[]{:S(2)}) copy-start(s32[256,2]{0,1:T(2,128)} %param.18) | copy-start | bytes 6148
  30.1 9.3 %collective-permute-start.5 = (bf16[64,1536]{1,0:T(8,128)(2,1)S(1)}, bf16[64,1536]{1,0:T(8,128)(2,1)}, u32[]{:S(2)}, u32[]{:S(2)}) collective-permute-start(bf16[64,1536]{1,0:T(8,128)(2,1)S(1)} %fusion.51), channel_id=1, source_target_pairs={{0,4},{4,0},{8,12},{12,8},{1,5},{5,1},{9,13},{13,9},{2,6},{6,2},{1... | collective-permute-start | bytes 589832 | tf_op jit(solution)/shard_map/ppermute | solution.py:95
  30.7 20.2 %collective-permute-start.3 = (bf16[256,768]{1,0:T(8,128)(2,1)}, bf16[256,768]{1,0:T(8,128)(2,1)}, u32[]{:S(2)}, u32[]{:S(2)}) collective-permute-start(bf16[256,768]{1,0:T(8,128)(2,1)} %slice.85), channel_id=1, source_target_pairs={{0,1},{1,0},{2,3},{3,2},{4,5},{5,4},{6,7},{7,6},{8,9},{9,8},{10,11... | collective-permute-start | bytes 1179656 | tf_op jit(solution)/shard_map/ppermute | solution.py:129
  32.0 1.0 copy-start.18
  33.0 17.9 %copy-start.3 = (f32[2,2,128,128]{2,3,1,0:T(8,128)}, f32[2,2,128,128]{2,3,1,0:T(8,128)S(1)}, u32[]{:S(2)}) copy-start(f32[2,2,128,128]{2,3,1,0:T(8,128)S(1)} %convolution_divide_fusion) | copy-start | bytes 786436
  33.1 8.0 %collective-permute-start.18 = (bf16[64,1536]{1,0:T(8,128)(2,1)}, bf16[64,1536]{1,0:T(8,128)(2,1)S(1)}, u32[]{:S(2)}, u32[]{:S(2)}) collective-permute-start(bf16[64,1536]{1,0:T(8,128)(2,1)} %collective-permute-done.17), channel_id=1, source_target_pairs={{0,2},{1,3},{2,0},{3,1},{4,6},{5,7},{6,4},{7,5},{8,10},{9,11},{10,... | collective-permute-start | bytes 589832 | tf_op jit(solution)/shard_map/ppermute | solution.py:113
  34.8 16.1 %copy-start.5 = (bf16[256,1536]{1,0:T(8,128)(2,1)S(1)}, bf16[256,1536]{1,0:T(8,128)(2,1)}, u32[]{:S(2)}) copy-start(bf16[256,1536]{1,0:T(8,128)(2,1)} %convolution_convert_fusion.3) | copy-start | bytes 2359300
  35.7 9.7 %collective-permute-start.12 = (bf16[64,1536]{1,0:T(8,128)(2,1)}, bf16[64,1536]{1,0:T(8,128)(2,1)S(1)}, u32[]{:S(2)}, u32[]{:S(2)}) collective-permute-start(bf16[64,1536]{1,0:T(8,128)(2,1)} %collective-permute-done.11), channel_id=1, source_target_pairs={{0,2},{1,3},{2,0},{3,1},{4,6},{5,7},{6,4},{7,5},{8,10},{9,11},{10,... | collective-permute-start | bytes 589832 | tf_op jit(solution)/shard_map/ppermute | solution.py:113
  39.4 9.8 %collective-permute-start.6 = (bf16[64,1536]{1,0:T(8,128)(2,1)}, bf16[64,1536]{1,0:T(8,128)(2,1)S(1)}, u32[]{:S(2)}, u32[]{:S(2)}) collective-permute-start(bf16[64,1536]{1,0:T(8,128)(2,1)} %collective-permute-done.5), channel_id=1, source_target_pairs={{0,2},{1,3},{2,0},{3,1},{4,6},{5,7},{6,4},{7,5},{8,10},{9,11},{10,... | collective-permute-start | bytes 589832 | tf_op jit(solution)/shard_map/ppermute | solution.py:113
  42.2 12.2 %collective-permute-start.19 = (bf16[128,1536]{1,0:T(8,128)(2,1)S(1)}, bf16[128,1536]{1,0:T(8,128)(2,1)S(1)}, u32[]{:S(2)}, u32[]{:S(2)}) collective-permute-start(bf16[128,1536]{1,0:T(8,128)(2,1)S(1)} %pad_maximum_fusion.25), channel_id=1, source_target_pairs={{0,1},{1,0},{2,3},{3,2},{4,5},{5,4},{6,7},{7,6},{8,9},{9,8},{10,11... | collective-permute-start | bytes 1179656 | tf_op jit(solution)/shard_map/ppermute | solution.py:113
  47.2 8.2 %copy-start.25 = (bf16[1,1536,768]{2,1,0:T(8,128)(2,1)S(1)}, bf16[1,1536,768]{2,1,0:T(8,128)(2,1)}, u32[]{:S(2)}) copy-start(bf16[1,1536,768]{2,1,0:T(8,128)(2,1)} %param.21) | copy-start | bytes 7077892
  47.2 16.8 %collective-permute-start.13 = (bf16[128,1536]{1,0:T(8,128)(2,1)}, bf16[128,1536]{1,0:T(8,128)(2,1)}, u32[]{:S(2)}, u32[]{:S(2)}) collective-permute-start(bf16[128,1536]{1,0:T(8,128)(2,1)} %pad_maximum_fusion.24), channel_id=1, source_target_pairs={{0,1},{1,0},{2,3},{3,2},{4,5},{5,4},{6,7},{7,6},{8,9},{9,8},{10,11... | collective-permute-start | bytes 1179656 | tf_op jit(solution)/shard_map/ppermute | solution.py:113
  50.9 23.7 %collective-permute-start.7 = (bf16[128,1536]{1,0:T(8,128)(2,1)}, bf16[128,1536]{1,0:T(8,128)(2,1)}, u32[]{:S(2)}, u32[]{:S(2)}) collective-permute-start(bf16[128,1536]{1,0:T(8,128)(2,1)} %pad_maximum_fusion.23), channel_id=1, source_target_pairs={{0,1},{1,0},{2,3},{3,2},{4,5},{5,4},{6,7},{7,6},{8,9},{9,8},{10,11... | collective-permute-start | bytes 1179656 | tf_op jit(solution)/shard_map/ppermute | solution.py:113
  52.7 51.4 %collective-permute-start.4 = (bf16[256,384]{1,0:T(8,128)(2,1)}, bf16[256,384]{1,0:T(8,128)(2,1)}, u32[]{:S(2)}, u32[]{:S(2)}) collective-permute-start(bf16[256,384]{1,0:T(8,128)(2,1)} %slice.87), channel_id=1, source_target_pairs={{0,2},{1,3},{2,0},{3,1},{4,6},{5,7},{6,4},{7,5},{8,10},{9,11},{10,... | collective-permute-start | bytes 589832 | tf_op jit(solution)/shard_map/ppermute | solution.py:129
  54.5 0.8 copy-start.11
  54.5 0.9 copy-start.12
  61.8 4.2 %copy-start.26 = (bf16[1,1536,768]{2,1,0:T(8,128)(2,1)S(1)}, bf16[1,1536,768]{2,1,0:T(8,128)(2,1)}, u32[]{:S(2)}) copy-start(bf16[1,1536,768]{2,1,0:T(8,128)(2,1)} %param.21) | copy-start | bytes 7077892
  63.7 20.7 %collective-permute-start.20 = (bf16[256,768]{1,0:T(8,128)(2,1)}, bf16[256,768]{1,0:T(8,128)(2,1)}, u32[]{:S(2)}, u32[]{:S(2)}) collective-permute-start(bf16[256,768]{1,0:T(8,128)(2,1)} %slice.97), channel_id=1, source_target_pairs={{0,1},{1,0},{2,3},{3,2},{4,5},{5,4},{6,7},{7,6},{8,9},{9,8},{10,11... | collective-permute-start | bytes 1179656 | tf_op jit(solution)/shard_map/ppermute | solution.py:129
  65.1 0.8 copy-start.13
  65.1 0.9 copy-start.14
  72.4 4.2 %copy-start.27 = (bf16[1,1536,768]{2,1,0:T(8,128)(2,1)S(1)}, bf16[1,1536,768]{2,1,0:T(8,128)(2,1)}, u32[]{:S(2)}) copy-start(bf16[1,1536,768]{2,1,0:T(8,128)(2,1)} %param.21) | copy-start | bytes 7077892
  74.3 11.8 %collective-permute-start.14 = (bf16[256,768]{1,0:T(8,128)(2,1)}, bf16[256,768]{1,0:T(8,128)(2,1)}, u32[]{:S(2)}, u32[]{:S(2)}) collective-permute-start(bf16[256,768]{1,0:T(8,128)(2,1)} %slice.93), channel_id=1, source_target_pairs={{0,1},{1,0},{2,3},{3,2},{4,5},{5,4},{6,7},{7,6},{8,9},{9,8},{10,11... | collective-permute-start | bytes 1179656 | tf_op jit(solution)/shard_map/ppermute | solution.py:129
  75.7 0.7 copy-start.9
  75.7 0.9 copy-start.10
  78.2 6.2 %copy-start.6 = (bf16[256,1536]{1,0:T(8,128)(2,1)S(1)}, bf16[256,1536]{1,0:T(8,128)(2,1)}, u32[]{:S(2)}) copy-start(bf16[256,1536]{1,0:T(8,128)(2,1)} %convolution_convert_fusion) | copy-start | bytes 2359300
  83.0 3.1 %copy-start.7 = (bf16[256,1536]{1,0:T(8,128)(2,1)S(1)}, bf16[256,1536]{1,0:T(8,128)(2,1)}, u32[]{:S(2)}) copy-start(bf16[256,1536]{1,0:T(8,128)(2,1)} %convolution_convert_fusion.1) | copy-start | bytes 2359300
  83.0 5.9 %copy-start.8 = (bf16[256,1536]{1,0:T(8,128)(2,1)S(1)}, bf16[256,1536]{1,0:T(8,128)(2,1)}, u32[]{:S(2)}) copy-start(bf16[256,1536]{1,0:T(8,128)(2,1)} %convolution_convert_fusion.2) | copy-start | bytes 2359300
  84.1 4.8 %collective-permute-start.8 = (bf16[256,768]{1,0:T(8,128)(2,1)S(1)}, bf16[256,768]{1,0:T(8,128)(2,1)S(1)}, u32[]{:S(2)}, u32[]{:S(2)}) collective-permute-start(bf16[256,768]{1,0:T(8,128)(2,1)S(1)} %slice.89), channel_id=1, source_target_pairs={{0,1},{1,0},{2,3},{3,2},{4,5},{5,4},{6,7},{7,6},{8,9},{9,8},{10,11... | collective-permute-start | bytes 1179656 | tf_op jit(solution)/shard_map/ppermute | solution.py:129
  85.6 17.7 %copy-start.4 = (f32[2,2,128,128]{2,3,1,0:T(8,128)S(1)}, f32[2,2,128,128]{2,3,1,0:T(8,128)}, u32[]{:S(2)}) copy-start(f32[2,2,128,128]{2,3,1,0:T(8,128)} %copy-done.3) | copy-start | bytes 786436
  85.6 17.7 %copy-start.19 = (f32[2]{0:T(128)S(1)}, f32[2]{0:T(128)}, u32[]{:S(2)}) copy-start(f32[2]{0:T(128)} %param.15) | copy-start | bytes 28
  85.6 17.7 %copy-start.24 = (f32[128]{0:T(128)S(1)}, f32[128]{0:T(128)}, u32[]{:S(2)}) copy-start(f32[128]{0:T(128)} %param.16) | copy-start | bytes 1540
  85.6 7.8 %collective-permute-start.21 = (bf16[256,384]{1,0:T(8,128)(2,1)S(1)}, bf16[256,384]{1,0:T(8,128)(2,1)S(1)}, u32[]{:S(2)}, u32[]{:S(2)}) collective-permute-start(bf16[256,384]{1,0:T(8,128)(2,1)S(1)} %slice.99), channel_id=1, source_target_pairs={{0,2},{1,3},{2,0},{3,1},{4,6},{5,7},{6,4},{7,5},{8,10},{9,11},{10,... | collective-permute-start | bytes 589832 | tf_op jit(solution)/shard_map/ppermute | solution.py:129
  87.2 26.1 %copy-start.17 = (f32[256]{0:T(256)S(1)}, f32[256]{0:T(256)}, u32[]{:S(2)}) copy-start(f32[256]{0:T(256)} %get-tuple-element.9) | copy-start | bytes 3076
  87.2 26.1 %copy-start.20 = (pred[256]{0:T(512)(128)(4,1)S(1)}, pred[256]{0:T(512)(128)(4,1)}, u32[]{:S(2)}) copy-start(pred[256]{0:T(512)(128)(4,1)} %get-tuple-element.10) | copy-start | bytes 772
  87.2 26.1 %copy-start.21 = (pred[256]{0:T(512)(128)(4,1)S(1)}, pred[256]{0:T(512)(128)(4,1)}, u32[]{:S(2)}) copy-start(pred[256]{0:T(512)(128)(4,1)} %get-tuple-element.11) | copy-start | bytes 772
  87.2 26.1 %copy-start.22 = (pred[256]{0:T(512)(128)(4,1)S(1)}, pred[256]{0:T(512)(128)(4,1)}, u32[]{:S(2)}) copy-start(pred[256]{0:T(512)(128)(4,1)} %get-tuple-element.12) | copy-start | bytes 772
  87.2 26.1 %copy-start.23 = (pred[256]{0:T(512)(128)(4,1)S(1)}, pred[256]{0:T(512)(128)(4,1)}, u32[]{:S(2)}) copy-start(pred[256]{0:T(512)(128)(4,1)} %get-tuple-element.13) | copy-start | bytes 772
  87.2 10.5 %collective-permute-start.15 = (bf16[256,384]{1,0:T(8,128)(2,1)S(1)}, bf16[256,384]{1,0:T(8,128)(2,1)S(1)}, u32[]{:S(2)}, u32[]{:S(2)}) collective-permute-start(bf16[256,384]{1,0:T(8,128)(2,1)S(1)} %slice.95), channel_id=1, source_target_pairs={{0,2},{1,3},{2,0},{3,1},{4,6},{5,7},{6,4},{7,5},{8,10},{9,11},{10,... | collective-permute-start | bytes 589832 | tf_op jit(solution)/shard_map/ppermute | solution.py:129
  89.1 12.1 %collective-permute-start.9 = (bf16[256,384]{1,0:T(8,128)(2,1)S(1)}, bf16[256,384]{1,0:T(8,128)(2,1)S(1)}, u32[]{:S(2)}, u32[]{:S(2)}) collective-permute-start(bf16[256,384]{1,0:T(8,128)(2,1)S(1)} %slice.91), channel_id=1, source_target_pairs={{0,2},{1,3},{2,0},{3,1},{4,6},{5,7},{6,4},{7,5},{8,10},{9,11},{10,... | collective-permute-start | bytes 589832 | tf_op jit(solution)/shard_map/ppermute | solution.py:129
  94.2 10.0 %collective-permute-start.22 = (bf16[256,384]{1,0:T(8,128)(2,1)}, bf16[256,384]{1,0:T(8,128)(2,1)S(1)}, u32[]{:S(2)}, u32[]{:S(2)}) collective-permute-start(bf16[256,384]{1,0:T(8,128)(2,1)} %add_convert_fusion.5), channel_id=1, source_target_pairs={{0,12},{4,8},{8,4},{12,0},{1,13},{5,9},{9,5},{13,1},{2,14},{6,10},... | collective-permute-start | bytes 589832 | tf_op jit(solution)/shard_map/ppermute | solution.py:138
  98.5 14.8 %collective-permute-start.16 = (bf16[256,384]{1,0:T(8,128)(2,1)}, bf16[256,384]{1,0:T(8,128)(2,1)S(1)}, u32[]{:S(2)}, u32[]{:S(2)}) collective-permute-start(bf16[256,384]{1,0:T(8,128)(2,1)} %add_convert_fusion.6), channel_id=1, source_target_pairs={{0,8},{4,12},{8,0},{12,4},{1,9},{5,13},{9,1},{13,5},{2,10},{6,14},... | collective-permute-start | bytes 589832 | tf_op jit(solution)/shard_map/ppermute | solution.py:138
  101.9 11.4 %collective-permute-start.10 = (bf16[256,384]{1,0:T(8,128)(2,1)}, bf16[256,384]{1,0:T(8,128)(2,1)S(1)}, u32[]{:S(2)}, u32[]{:S(2)}) collective-permute-start(bf16[256,384]{1,0:T(8,128)(2,1)} %add_convert_fusion.7), channel_id=1, source_target_pairs={{0,4},{4,0},{8,12},{12,8},{1,5},{5,1},{9,13},{13,9},{2,6},{6,2},{1... | collective-permute-start | bytes 589832 | tf_op jit(solution)/shard_map/ppermute | solution.py:138

commit v2 on v1

--- a/solution.py
+++ b/solution.py
@@ -1,6 +1,10 @@
+import math
+
 import jax
 import jax.numpy as jnp
 from jax import lax
+from jax.experimental import pallas as pl
+from jax.experimental.pallas import tpu as pltpu
 from jax.sharding import PartitionSpec as P
 
 
@@ -77,6 +81,174 @@
     ).astype(jnp.bfloat16)
 
 
+def rms_rows(token_block, gain_row):
+    token_float = token_block.astype(jnp.float32)
+    scale = lax.rsqrt(jnp.mean(token_float * token_float, axis=1, keepdims=True) + 1e-06)
+    return (token_float * scale * gain_row).astype(jnp.bfloat16)
+
+
+def call(kernel, name, inputs, spaces, out_shapes, scratch, flops, grant):
+    moved = sum(x.size * x.dtype.itemsize for x in inputs)
+    moved += sum(math.prod(o.shape) * o.dtype.itemsize for o in out_shapes)
+    return pl.pallas_call(
+        kernel,
+        name=name,
+        out_shape=out_shapes,
+        in_specs=[pl.BlockSpec(memory_space=s) for s in spaces],
+        out_specs=[pl.BlockSpec(memory_space=pltpu.VMEM)] * len(out_shapes),
+        scratch_shapes=scratch,
+        cost_estimate=pl.CostEstimate(flops=flops, bytes_accessed=moved, transcendentals=0),
+        compiler_params=pltpu.CompilerParams(vmem_limit_bytes=grant),
+    )(*inputs)
+
+
+def own_piece(tokens, part, moe_gain, piece_rows):
+    width = tokens.shape[1]
+
+    def kernel(part_ref, token_ref, gain_ref, out_ref):
+        at = pl.multiple_of(part_ref[0] * piece_rows, piece_rows)
+        out_ref[...] = rms_rows(token_ref[pl.ds(at, piece_rows), :], gain_ref[...])
+
+    return call(
+        kernel,
+        "own_piece",
+        (part.reshape(1), tokens, moe_gain.reshape(1, width)),
+        (pltpu.SMEM, pltpu.VMEM, pltpu.VMEM),
+        [jax.ShapeDtypeStruct((piece_rows, width), jnp.bfloat16)],
+        [],
+        8 * piece_rows * width,
+        4 << 20,
+    )[0]
+
+
+def expert_kernel(pieces, places, blocks, gain, mats, name):
+    gate_mat, up_mat, down_mat = mats
+    width, units = gate_mat.shape
+    block_count = blocks.shape[0]
+    block = width // block_count
+    part_rows = pieces[0].shape[0]
+    row_count = part_rows * len(pieces)
+    half = block_count // 2
+    chunk = math.gcd(units, 256)
+
+    def kernel(*refs):
+        place_ref, block_ref = refs[:2]
+        rest = refs[2:]
+        if gain is not None:
+            gain_ref, rest = rest[0], rest[1:]
+        piece_refs, rest = rest[: len(pieces)], rest[len(pieces) :]
+        gate_ref, up_ref, down_ref, send_ref, keep_ref, rows, hidden = rest
+        if gain is not None:
+            rows[...] = rms_rows(piece_refs[0][...], gain_ref[...])
+        else:
+            for index, ref in enumerate(piece_refs):
+                at = pl.multiple_of(place_ref[index] * part_rows, part_rows)
+                rows[pl.ds(at, part_rows), :] = ref[...]
+        for step in range(units // chunk):
+            columns = pl.ds(step * chunk, chunk)
+            gate = jnp.dot(rows[...], gate_ref[:, columns], preferred_element_type=jnp.float32)
+            upward = jnp.dot(rows[...], up_ref[:, columns], preferred_element_type=jnp.float32)
+            hidden[:, columns] = (gate / (1.0 + jnp.exp(-gate)) * upward).astype(jnp.bfloat16)
+        for index in range(block_count):
+            columns = pl.ds(pl.multiple_of(block_ref[index] * block, block), block)
+            out = jnp.dot(
+                hidden[...], down_ref[:, columns], preferred_element_type=jnp.float32
+            ).astype(jnp.bfloat16)
+            if index < half:
+                send_ref[:, index * block : (index + 1) * block] = out
+            else:
+                keep_ref[:, (index - half) * block : (index - half + 1) * block] = out
+
+    gains = () if gain is None else (gain.reshape(1, width),)
+    inputs = (places, blocks, *gains, *pieces, gate_mat, up_mat, down_mat)
+    spaces = (pltpu.SMEM,) * 2 + (pltpu.VMEM,) * (len(inputs) - 2)
+    shape = jax.ShapeDtypeStruct((row_count, half * block), jnp.bfloat16)
+    return call(
+        kernel,
+        name,
+        inputs,
+        spaces,
+        [shape, shape],
+        [pltpu.VMEM((row_count, width), jnp.bfloat16), pltpu.VMEM((row_count, units), jnp.bfloat16)],
+        6 * row_count * width * units,
+        20 << 20,
+    )
+
+
+def add_halves(kept, came, name):
+    row_count, columns = kept.shape
+    half = columns // 2
+
+    def kernel(kept_ref, came_ref, send_ref, keep_ref):
+        for ref, at in ((send_ref, 0), (keep_ref, half)):
+            one = kept_ref[:, at : at + half].astype(jnp.float32)
+            two = came_ref[:, at : at + half].astype(jnp.float32)
+            ref[...] = (one + two).astype(jnp.bfloat16)
+
+    shape = jax.ShapeDtypeStruct((row_count, half), jnp.bfloat16)
+    return call(
+        kernel,
+        name,
+        (kept, came),
+        (pltpu.VMEM,) * 2,
+        [shape, shape],
+        [],
+        row_count * columns,
+        4 << 20,
+    )
+
+
+def add_last(kept, came, name):
+    def kernel(kept_ref, came_ref, out_ref):
+        out_ref[...] = (
+            kept_ref[...].astype(jnp.float32) + came_ref[...].astype(jnp.float32)
+        ).astype(jnp.bfloat16)
+
+    return call(
+        kernel,
+        name,
+        (kept, came),
+        (pltpu.VMEM,) * 2,
+        [jax.ShapeDtypeStruct(kept.shape, jnp.bfloat16)],
+        [],
+        kept.size,
+        4 << 20,
+    )[0]
+
+
+def weighted_sum(route_ids, route_weights, ep_index, own, results):
+    row_count, columns = results[0].shape
+    top_count = route_ids.shape[1]
+
+    def kernel(index_ref, id_ref, weight_ref, kept_ref, came_ref, *refs):
+        result_refs, out_ref = refs[:-1], refs[-1]
+        total = jnp.zeros((row_count, columns), jnp.float32)
+        for step in range(len(results) + 1):
+            expert = index_ref[0] ^ step
+            if step == 0:
+                result = kept_ref[...].astype(jnp.float32) + came_ref[...].astype(jnp.float32)
+                result = result.astype(jnp.bfloat16).astype(jnp.float32)
+            else:
+                result = result_refs[step - 1][...].astype(jnp.float32)
+            for choice in range(top_count):
+                named = id_ref[:, choice : choice + 1] == expert
+                term = result * weight_ref[:, choice : choice + 1]
+                total += jnp.where(named, term, 0.0)
+        out_ref[...] = total.astype(jnp.bfloat16)
+
+    inputs = (ep_index.reshape(1), route_ids, route_weights, *own, *results)
+    return call(
+        kernel,
+        "weighted_sum",
+        inputs,
+        (pltpu.SMEM,) + (pltpu.VMEM,) * (len(inputs) - 1),
+        [jax.ShapeDtypeStruct((row_count, columns), jnp.bfloat16)],
+        [],
+        8 * row_count * columns,
+        8 << 20,
+    )[0]
+
+
 def experts_whole(tokens, route_ids, route_weights, moe_gain, w_gate, w_up, w_down):
     row_count, width = tokens.shape
     ep_size = lax.axis_size("ep")
@@ -85,64 +257,54 @@
     tp_index = lax.axis_index("tp")
     steps = halving_steps(tp_size)
     piece_rows = row_count // tp_size
-    part = jnp.zeros((), jnp.int32)
-    for place, step in enumerate(steps):
-        part = part + jnp.where(tp_index & step != 0, 1 << place, 0)
-    mine = normalize(
-        lax.dynamic_slice_in_dim(tokens, part * piece_rows, piece_rows, 0), moe_gain
-    )
+
+    def reversed_bits(index):
+        part = jnp.zeros((), jnp.int32)
+        for place, step in enumerate(steps):
+            part = part + jnp.where(index & step != 0, 1 << place, 0)
+        return part
+
+    part = reversed_bits(tp_index)
+    mine = own_piece(tokens, part, moe_gain, piece_rows)
     arrivals = [
         lax.ppermute(mine, "ep", xor_pairs(ep_size, step)) for step in range(1, ep_size)
     ]
-    gate_mat, up_mat = w_gate[0], w_up[0]
-    slice_width = width // tp_size
-    order = []
+    mats = (w_gate[0], w_up[0], w_down[0])
+    blocks = []
     for place in range(tp_size):
         target = tp_index
         for bit, step in enumerate(steps):
             if not (place >> bit) & 1:
                 target = target ^ step
-        order.append(target)
-    down_mat = jnp.concatenate(
-        [lax.dynamic_slice_in_dim(w_down[0], t * slice_width, slice_width, 1) for t in order],
-        axis=1,
-    )
+        blocks.append(target)
+    blocks = jnp.stack(blocks)
 
     def all_rows(piece):
+        pieces, flips = [piece], [0]
         for step in steps:
-            other = lax.ppermute(piece, "tp", xor_pairs(tp_size, step))
-            low = tp_index & step == 0
-            piece = jnp.concatenate(
-                [jnp.where(low, piece, other), jnp.where(low, other, piece)], axis=0
-            )
-        return piece
-
-    def expert(rows):
-        gate = jnp.dot(rows, gate_mat, preferred_element_type=jnp.float32)
-        upward = jnp.dot(rows, up_mat, preferred_element_type=jnp.float32)
-        hidden = (jax.nn.silu(gate) * upward).astype(jnp.bfloat16)
-        partial = jnp.dot(hidden, down_mat, preferred_element_type=jnp.float32).astype(
-            jnp.bfloat16
-        )
+            pieces = pieces + [lax.ppermute(p, "tp", xor_pairs(tp_size, step)) for p in pieces]
+            flips = flips + [f ^ step for f in flips]
+        places = jnp.stack([reversed_bits(tp_index ^ f) for f in flips])
+        return pieces, places
+
+    def reduced(send, keep, name, last):
         for step in reversed(steps):
-            half = partial.shape[1] // 2
-            other = lax.ppermute(partial[:, :half], "tp", xor_pairs(tp_size, step))
-            partial = (
-                partial[:, half:].astype(jnp.float32) + other.astype(jnp.float32)
-            ).astype(jnp.bfloat16)
-        return partial
-
-    results = [expert(normalize(tokens, moe_gain))]
+            came = lax.ppermute(send, "tp", xor_pairs(tp_size, step))
+            if step == steps[0]:
+                return add_last(keep, came, name + "_last") if last else (keep, came)
+            send, keep = add_halves(keep, came, name + f"_{step}")
+
+    places = jnp.zeros((1,), jnp.int32)
+    own = reduced(
+        *expert_kernel([tokens], places, blocks, moe_gain, mats, "expert_0"), "add_0", False
+    )
+    results = []
     for step in range(1, ep_size):
-        done = expert(all_rows(arrivals[step - 1]))
+        pieces, places = all_rows(arrivals[step - 1])
+        name = f"expert_{step}"
+        done = reduced(*expert_kernel(pieces, places, blocks, None, mats, name), f"add_{step}", True)
         results.append(lax.ppermute(done, "ep", xor_pairs(ep_size, step)))
-    total = jnp.zeros((row_count, slice_width), jnp.float32)
-    for step in range(ep_size):
-        named = route_ids == (ep_index ^ step)
-        weight = jnp.sum(jnp.where(named, route_weights, 0.0), axis=1, keepdims=True)
-        here = jnp.any(named, axis=1, keepdims=True)
-        total = total + jnp.where(here, results[step].astype(jnp.float32) * weight, 0.0)
-    return total.astype(jnp.bfloat16)
+    return weighted_sum(route_ids, route_weights, ep_index, own, results)
 
 
 def experts_slots(tokens, route_ids, route_weights, moe_gain, w_gate, w_up, w_down):
@@ -207,7 +369,10 @@
         and w_gate.shape[0] == 1
         and power_of_two(ep_size)
         and power_of_two(tp_size)
-        and row_count % tp_size == 0
+        and tp_size > 1
+        and row_count % (16 * tp_size) == 0
+        and w_gate.shape[2] % 128 == 0
+        and tokens.shape[1] % (128 * tp_size) == 0
     )
     chosen = experts_whole if whole else experts_slots
     return chosen(tokens, route_ids, route_weights, moe_gain, w_gate, w_up, w_down)

time: 116 us -> 99.8 us (0.86)
  matrix products: 28.2 us -> 2.86 us
  other arithmetic: 21.2 us -> 1.51 us
  Pallas kernels: 0 us -> 17.8 us
  local copies, waits for them, and re-layouts: 15.6 us -> 22 us
  starting transfers between devices: 27 us -> 30 us
  waiting for transfers between devices: 22.2 us -> 23.9 us
    dot_general x8 -> x0, matrix products: 27.5 us -> none  [the longest x4 18.7 us: expert(): jnp.dot(hidden, down_mat, preferred_element_type=jnp.float32)]
    pallas_call x0 -> x13, Pallas kernels: none -> 17.8 us  [call(): pl.pallas_call(kernel, name=name, out_shape=out_shapes, in_specs=[pl.Bloc...]
    unnamed x59 -> x49, local copies, waits for them, and re-layouts: 5.42 us -> 16.7 us
    convert_element_type x9 -> x0, other arithmetic: 8.58 us -> none  [the longest x7 5.56 us: expert(): partial = (partial[:, half:].astype(jnp.float32) + other.astype(jnp.float...]
    ppermute x3, waiting for transfers between devices: 0.01 us -> 7.64 us  [gathered(): pieces.append(lax.ppermute(piece, 'ep', xor_pairs(size, step)))]
    slice x8 -> x0, local copies, waits for them, and re-layouts: 7.56 us -> none  [expert(): other = lax.ppermute(partial[:, :half], 'tp', xor_pairs(tp_size, step))]
    select_n x6 -> x0, other arithmetic: 5.25 us -> none  [all_rows(): jnp.where(low, piece, other)]
    reduce_sum x3 -> x0, other arithmetic: 3.71 us -> none  [the longest x2 2.43 us: normalize(): jnp.mean(token_float * token_float, axis=1, keepdims=True) + 1e-06]
  transfers between devices with their start and end apart: 23 -> 26, of which waited for: 8 -> 7; matrix products, arithmetic and copies ran while one was open for 51% -> 13% of each run, Pallas kernels for 0% -> 16%
where the time goes in v2:
time: 99.8 us; the launch traced here: 99 us
  starting transfers between devices  30 us (30%)
  waiting for transfers between devices  23.9 us (24%)
  local copies, waits for them, and re-layouts  22 us (22%)
  Pallas kernels  17.8 us (18%)
  matrix products  2.86 us (3%)
  other arithmetic  1.51 us (2%)
    pallas_call x13, Pallas kernels, call(): pl.pallas_call(kernel, name=name, out_shape=out_shapes, in_specs=[pl.Bloc...  17.8 us
    unnamed x49, local copies, waits for them, and re-layouts  16.7 us
    ppermute x3, starting transfers between devices, experts_whole(): results.append(lax.ppermute(done, 'ep', xor_pairs(ep_size, step)))  9.95 us
    ppermute x3, waiting for transfers between devices, gathered(): pieces.append(lax.ppermute(piece, 'ep', xor_pairs(size, step)))  7.64 us
    ppermute x3, waiting for transfers between devices, experts_whole(): results.append(lax.ppermute(done, 'ep', xor_pairs(ep_size, step)))  7.4 us
    ppermute x3, starting transfers between devices, experts_whole(): lax.ppermute(mine, 'ep', xor_pairs(ep_size, step))  5.71 us
    ppermute x8, starting transfers between devices, reduced(): came = lax.ppermute(send, 'tp', xor_pairs(tp_size, step))  5.39 us
    ppermute x9, waiting for transfers between devices, all_rows(): lax.ppermute(p, 'tp', xor_pairs(tp_size, step))  4.86 us
  transfers between devices with their start and end apart: 26, of which 7 were waited for; matrix products, arithmetic and copies ran while one was open for 13% of the time, Pallas kernels for 16%

profile of v2, /device:TPU:0, one launch (start us, length us, event | category | flops | bytes accessed | tf_op | source)
XLA Modules:
  0.0 99.0 jit_solution(14064248817338514331)
XLA Ops:
  0.6 0.7 reshape.39.refs_2_.gain_ref
  1.3 1.1 %copy-done.6 = bf16[256,1536]{1,0:T(8,128)(2,1)S(1)} copy-done((bf16[256,1536]{1,0:T(8,128)(2,1)S(1)}, bf16[256,1536]{1,0:T(8,128)(2,1)}, u32[]{:S(2)}) %copy-start.6) | copy-done | bytes 786456
  2.5 0.1 own_piece.1
  2.6 5.1 %collective-permute-start.19 = (bf16[64,1536]{1,0:T(8,128)(2,1)S(1)}, bf16[64,1536]{1,0:T(8,128)(2,1)S(1)}, u32[]{:S(2)}, u32[]{:S(2)}) collective-permute-start(bf16[64,1536]{1,0:T(8,128)(2,1)S(1)} %own_piece.1), channel_id=1, source_target_pairs={{0,12},{4,8},{8,4},{12,0},{1,13},{5,9},{9,5},{13,1},{2,14},{6,10},... | collective-permute-start | bytes 589832 | tf_op jit(solution)/shard_map/ppermute | solution.py:270
  7.8 0.8 constant_dynamic-update-slice_fusion.1
  8.6 0.8 constant_dynamic-update-slice_fusion
  9.5 0.6 collective-permute-start
  10.1 2.3 %collective-permute-start.1 = (bf16[128,512]{1,0:T(8,128)(2,1)S(1)}, bf16[128,512]{1,0:T(8,128)(2,1)}, u32[]{:S(2)}, u32[]{:S(2)}) collective-permute-start(bf16[128,512]{1,0:T(8,128)(2,1)S(1)} %constant_dynamic-update-slice_fusion), channel_id=1, source_target_pairs={{0,8},{4,12},{8,0},{12,4},{1,9},{5,13},{9,1},{13,5},{2,10},{6,14},... | collective-permute-start | bytes 393224 | tf_op jit(solution)/shard_map/ppermute | solution.py:32
  12.4 1.5 %collective-permute-start.2 = (bf16[128,512]{1,0:T(8,128)(2,1)S(1)}, bf16[128,512]{1,0:T(8,128)(2,1)}, u32[]{:S(2)}, u32[]{:S(2)}) collective-permute-start(bf16[128,512]{1,0:T(8,128)(2,1)S(1)} %constant_dynamic-update-slice_fusion), channel_id=1, source_target_pairs={{0,12},{4,8},{8,4},{12,0},{1,13},{5,9},{9,5},{13,1},{2,14},{6,10},... | collective-permute-start | bytes 393224 | tf_op jit(solution)/shard_map/ppermute | solution.py:32
  13.8 0.1 pad_add_fusion
  13.9 1.7 %copy-done = bf16[1,1536,768]{2,1,0:T(8,128)(2,1)S(1)} copy-done((bf16[1,1536,768]{2,1,0:T(8,128)(2,1)S(1)}, bf16[1,1536,768]{2,1,0:T(8,128)(2,1)}, u32[]{:S(2)}) %copy-start) | copy-done | bytes 2359320
  15.6 1.7 %copy-done.2 = bf16[1,1536,768]{2,1,0:T(8,128)(2,1)S(1)} copy-done((bf16[1,1536,768]{2,1,0:T(8,128)(2,1)S(1)}, bf16[1,1536,768]{2,1,0:T(8,128)(2,1)}, u32[]{:S(2)}) %copy-start.2) | copy-done | bytes 2359320
  17.3 1.7 %copy-done.4 = bf16[1,768,1536]{2,1,0:T(8,128)(2,1)S(1)} copy-done((bf16[1,768,1536]{2,1,0:T(8,128)(2,1)S(1)}, bf16[1,768,1536]{2,1,0:T(8,128)(2,1)}, u32[]{:S(2)}) %copy-start.4) | copy-done | bytes 2359320
  18.9 1.1 %copy-done.7 = bf16[256,1536]{1,0:T(8,128)(2,1)S(1)} copy-done((bf16[256,1536]{1,0:T(8,128)(2,1)S(1)}, bf16[256,1536]{1,0:T(8,128)(2,1)}, u32[]{:S(2)}) %copy-start.7) | copy-done | bytes 786456
  20.1 2.9 %expert_0.1 = (bf16[256,768]{1,0:T(8,128)(2,1)S(1)}, bf16[256,768]{1,0:T(8,128)(2,1)S(1)}) custom-call(s32[1]{0:T(128)} %constant.11.clone.1.refs_0_, s32[4]{0:T(128)S(1)} %get-tuple-element.42.refs_1_, f32[1,1536]{1,0:T(1,128)S(1)} %reshape.39.refs_2_.gain_ref, bf16[256,1536]{1,0:T(8,128)(2,1)S(1)} %copy-done.7, bf16[1536,768]{1,0:T(8,128)(2,1)S(1)} %bitcast.47, ...), custom_call_target="tpu_custom_call" | custom-call | flops 1811939328 | bytes 8656916 | tf_op jit(solution)/shard_map/expert_0/pallas_call | solution.py:93
  23.0 0.8 copy-done.16
  23.8 0.1 copy.27.id_ref
  23.9 0.1 copy.28.weight_ref
  24.0 1.7 %copy.23 = bf16[128,256]{0,1:T(8,128)(2,1)} copy(bf16[128,256]{1,0:T(8,128)(2,1)} %param.12) | data formatting | bytes 131072 | tf_op args[0]
  25.8 0.6 collective-permute-start.5
  26.3 7.6 %collective-permute-done.1 = bf16[128,512]{1,0:T(8,128)(2,1)} collective-permute-done((bf16[128,512]{1,0:T(8,128)(2,1)S(1)}, bf16[128,512]{1,0:T(8,128)(2,1)}, u32[]{:S(2)}, u32[]{:S(2)}) %collective-permute-start.1) | collective-permute-done | bytes 131104 | tf_op jit(solution)/shard_map/ppermute | solution.py:32
  34.0 1.1 %pad_maximum_fusion = bf16[512,512]{1,0:T(8,128)(2,1)S(1)} fusion(bf16[128,512]{1,0:T(8,128)(2,1)} %collective-permute-done.2, bf16[128,512]{1,0:T(8,128)(2,1)} %collective-permute-done.1, bf16[128,512]{1,0:T(8,128)(2,1)} %collective-permute-done, bf16[128,512]{1,0:T(8,128)(2,1)S(1)} %constant_dynamic-update-slice_fusion), kind=kLoop, calls=%fused_computation.6 | loop fusion | flops 2097152 | bytes 1048576 | tf_op jit(solution)/shard_map/concatenate | solution.py:33
  35.1 1.6 %collective-permute-start.20 = (bf16[64,1536]{1,0:T(8,128)(2,1)S(1)}, bf16[64,1536]{1,0:T(8,128)(2,1)}, u32[]{:S(2)}, u32[]{:S(2)}) collective-permute-start(bf16[64,1536]{1,0:T(8,128)(2,1)S(1)} %collective-permute-done.19.refs_2_), channel_id=1, source_target_pairs={{0,2},{1,3},{2,0},{3,1},{4,6},{5,7},{6,4},{7,5},{8,10},{9,11},{10,... | collective-permute-start | bytes 589832 | tf_op jit(solution)/shard_map/ppermute | solution.py:285
  36.6 0.5 collective-permute-start.13
  37.2 0.8 fusion.7
  38.0 1.8 %copy.22 = bf16[512,256]{0,1:T(8,128)(2,1)} copy(bf16[512,256]{1,0:T(8,128)(2,1)} %get-tuple-element.38) | data formatting | bytes 524288 | tf_op jit(solution)/shard_map/slice | solution.py:45
  39.8 0.5 collective-permute-start.14
  40.3 1.5 %collective-permute-start.6 = (bf16[64,1536]{1,0:T(8,128)(2,1)}, bf16[64,1536]{1,0:T(8,128)(2,1)S(1)}, u32[]{:S(2)}, u32[]{:S(2)}) collective-permute-start(bf16[64,1536]{1,0:T(8,128)(2,1)} %collective-permute-done.5.refs_2_), channel_id=1, source_target_pairs={{0,2},{1,3},{2,0},{3,1},{4,6},{5,7},{6,4},{7,5},{8,10},{9,11},{10,... | collective-permute-start | bytes 589832 | tf_op jit(solution)/shard_map/ppermute | solution.py:285
  41.8 0.6 collective-permute-done.20.refs_3_
  42.4 3.4 %collective-permute-done.13.refs_3_ = bf16[64,1536]{1,0:T(8,128)(2,1)} collective-permute-done((bf16[64,1536]{1,0:T(8,128)(2,1)}, bf16[64,1536]{1,0:T(8,128)(2,1)}, u32[]{:S(2)}, u32[]{:S(2)}) %collective-permute-start.13) | collective-permute-done | bytes 196640 | tf_op jit(solution)/shard_map/ppermute | solution.py:285
  45.7 1.3 %fusion.8 = (f32[2,2,128]{2,1,0:T(2,128)S(1)}, f32[2,2,128,512]{2,3,1,0:T(8,128)S(1)}) fusion(bf16[512,2,2,64]{0,3,2,1:T(8,128)(2,1)} %bitcast.59, bf16[128,2,2,64]{0,3,2,1:T(8,128)(2,1)} %bitcast.62), kind=kOutput, calls=%fused_computation.20 | convolution fusion | flops 34078208 | bytes 1378304 | tf_op jit(solution)/shard_map/qhcd,khcd->hcqk/dot_general | solution.py:53
  47.1 0.6 collective-permute-start.3
  47.7 0.9 collective-permute-done.6.refs_3_
  48.6 0.5 collective-permute-start.8
  49.1 1.7 %copy-done.3 = bf16[1,1536,768]{2,1,0:T(8,128)(2,1)S(1)} copy-done((bf16[1,1536,768]{2,1,0:T(8,128)(2,1)S(1)}, bf16[1,1536,768]{2,1,0:T(8,128)(2,1)}, u32[]{:S(2)}) %copy-start.3) | copy-done | bytes 2359320
  50.8 1.7 %copy-done.5 = bf16[1,768,1536]{2,1,0:T(8,128)(2,1)S(1)} copy-done((bf16[1,768,1536]{2,1,0:T(8,128)(2,1)S(1)}, bf16[1,768,1536]{2,1,0:T(8,128)(2,1)}, u32[]{:S(2)}) %copy-start.5) | copy-done | bytes 2359320
  52.4 0.9 copy-done.15
  53.4 3.6 %expert_3.1 = (bf16[256,768]{1,0:T(8,128)(2,1)}, bf16[256,768]{1,0:T(8,128)(2,1)S(1)}) custom-call(s32[4]{0:T(128)S(1)} %get-tuple-element.43.refs_0_, s32[4]{0:T(128)S(1)} %get-tuple-element.42.refs_1_, bf16[64,1536]{1,0:T(8,128)(2,1)S(1)} %copy-done.15, bf16[64,1536]{1,0:T(8,128)(2,1)} %collective-permute-done.20.refs_3_, ...), custom_call_target="tpu_custom_call" | custom-call | flops 1811939328 | bytes 8650784 | tf_op jit(solution)/shard_map/expert_3/pallas_call | solution.py:93
  56.9 3.8 %expert_2.1 = (bf16[256,768]{1,0:T(8,128)(2,1)}, bf16[256,768]{1,0:T(8,128)(2,1)S(1)}) custom-call(s32[4]{0:T(128)S(1)} %get-tuple-element.43.refs_0_, s32[4]{0:T(128)S(1)} %get-tuple-element.42.refs_1_, bf16[64,1536]{1,0:T(8,128)(2,1)} %collective-permute-done.12.refs_2_, bf16[64,1536]{1,0:T(8,128)(2,1)} %collective-permute-done.13.refs_3_, ...), custom_call_target="tpu_custom_call" | custom-call | flops 1811939328 | bytes 8650784 | tf_op jit(solution)/shard_map/expert_2/pallas_call | solution.py:93
  60.7 0.4 collective-permute-start.16
  61.1 3.6 %expert_1.1 = (bf16[256,768]{1,0:T(8,128)(2,1)}, bf16[256,768]{1,0:T(8,128)(2,1)S(1)}) custom-call(s32[4]{0:T(128)S(1)} %get-tuple-element.43.refs_0_, s32[4]{0:T(128)S(1)} %get-tuple-element.42.refs_1_, bf16[64,1536]{1,0:T(8,128)(2,1)} %collective-permute-done.5.refs_2_, bf16[64,1536]{1,0:T(8,128)(2,1)S(1)} %collective-permute-done.6.refs_3_, ...), custom_call_target="tpu_custom_call" | custom-call | flops 1811939328 | bytes 8650784 | tf_op jit(solution)/shard_map/expert_1/pallas_call | solution.py:93
  64.7 0.7 copy-done.12
  65.4 0.2 collective-permute-start.9
  65.6 0.2 fusion.1
  65.7 1.1 %copy.24 = bf16[512,256]{0,1:T(8,128)(2,1)S(1)} copy(bf16[512,256]{1,0:T(8,128)(2,1)} %get-tuple-element.39) | data formatting | bytes 524288 | tf_op jit(solution)/shard_map/slice | solution.py:45
  66.9 1.5 %convolution_divide_fusion = f32[2,2,128,128]{2,3,1,0:T(8,128)S(1)} fusion(bf16[512,2,128,1]{0,2,3,1:T(8,128)(2,1)S(1)} %bitcast.61, f32[2,2,128,512]{2,3,1,0:T(8,128)} %copy-done.17, f32[2,2,128]{2,1,0:T(2,128)S(1)} %get-tuple-element.40, f32[2,2,128]{2,1,0:T(2,128)S(1)} %fusion.1), kind=kOutput, calls=%fused_computation.2 | convolution fusion | flops 67698688 | bytes 1576960 | tf_op jit(solution)/shard_map/hcqk,khe->hcqe/dot_general | solution.py:59
  68.4 0.1 multiply_reduce_fusion
  68.6 1.1 %add_3_1.1 = (bf16[256,384]{1,0:T(8,128)(2,1)S(1)}, bf16[256,384]{1,0:T(8,128)(2,1)S(1)}) custom-call(bf16[256,768]{1,0:T(8,128)(2,1)S(1)} %copy-done.9, bf16[256,768]{1,0:T(8,128)(2,1)} %collective-permute-done.23.came_ref), custom_call_target="tpu_custom_call" | custom-call | flops 196608 | bytes 1179648 | tf_op jit(solution)/shard_map/add_3_1/pallas_call | solution.py:93
  69.7 1.6 %collective-permute-start.24 = (bf16[256,384]{1,0:T(8,128)(2,1)S(1)}, bf16[256,384]{1,0:T(8,128)(2,1)S(1)}, u32[]{:S(2)}, u32[]{:S(2)}) collective-permute-start(bf16[256,384]{1,0:T(8,128)(2,1)S(1)} %get-tuple-element.33), channel_id=1, source_target_pairs={{0,2},{1,3},{2,0},{3,1},{4,6},{5,7},{6,4},{7,5},{8,10},{9,11},{10,... | collective-permute-start | bytes 589832 | tf_op jit(solution)/shard_map/ppermute | solution.py:292
  71.2 1.1 %add_2_1.1 = (bf16[256,384]{1,0:T(8,128)(2,1)S(1)}, bf16[256,384]{1,0:T(8,128)(2,1)S(1)}) custom-call(bf16[256,768]{1,0:T(8,128)(2,1)S(1)} %copy-done.11, bf16[256,768]{1,0:T(8,128)(2,1)} %collective-permute-done.16.came_ref), custom_call_target="tpu_custom_call" | custom-call | flops 196608 | bytes 1179648 | tf_op jit(solution)/shard_map/add_2_1/pallas_call | solution.py:93
  72.3 0.6 collective-permute-start.17
  72.9 0.1 add_1_1.1
  73.0 1.6 %collective-permute-start.10 = (bf16[256,384]{1,0:T(8,128)(2,1)S(1)}, bf16[256,384]{1,0:T(8,128)(2,1)S(1)}, u32[]{:S(2)}, u32[]{:S(2)}) collective-permute-start(bf16[256,384]{1,0:T(8,128)(2,1)S(1)} %get-tuple-element.25), channel_id=1, source_target_pairs={{0,2},{1,3},{2,0},{3,1},{4,6},{5,7},{6,4},{7,5},{8,10},{9,11},{10,... | collective-permute-start | bytes 589832 | tf_op jit(solution)/shard_map/ppermute | solution.py:292
  74.6 0.1 add_0_1.1
  74.7 0.6 collective-permute-start.4
  75.3 2.2 %collective-permute-done.24.came_ref = bf16[256,384]{1,0:T(8,128)(2,1)S(1)} collective-permute-done((bf16[256,384]{1,0:T(8,128)(2,1)S(1)}, bf16[256,384]{1,0:T(8,128)(2,1)S(1)}, u32[]{:S(2)}, u32[]{:S(2)}) %collective-permute-start.24) | collective-permute-done | bytes 196640 | tf_op jit(solution)/shard_map/ppermute | solution.py:292
  77.6 2.4 %collective-permute-start.25 = (bf16[256,384]{1,0:T(8,128)(2,1)S(1)}, bf16[256,384]{1,0:T(8,128)(2,1)S(1)}, u32[]{:S(2)}, u32[]{:S(2)}) collective-permute-start(bf16[256,384]{1,0:T(8,128)(2,1)S(1)} %add_3_last.1), channel_id=1, source_target_pairs={{0,12},{4,8},{8,4},{12,0},{1,13},{5,9},{9,5},{13,1},{2,14},{6,10},... | collective-permute-start | bytes 589832 | tf_op jit(solution)/shard_map/ppermute | solution.py:306
  79.9 1.8 %collective-permute-done.17.came_ref = bf16[256,384]{1,0:T(8,128)(2,1)S(1)} collective-permute-done((bf16[256,384]{1,0:T(8,128)(2,1)S(1)}, bf16[256,384]{1,0:T(8,128)(2,1)S(1)}, u32[]{:S(2)}, u32[]{:S(2)}) %collective-permute-start.17) | collective-permute-done | bytes 196640 | tf_op jit(solution)/shard_map/ppermute | solution.py:292
  81.8 4.3 %collective-permute-start.18 = (bf16[256,384]{1,0:T(8,128)(2,1)S(1)}, bf16[256,384]{1,0:T(8,128)(2,1)S(1)}, u32[]{:S(2)}, u32[]{:S(2)}) collective-permute-start(bf16[256,384]{1,0:T(8,128)(2,1)S(1)} %add_2_last.1), channel_id=1, source_target_pairs={{0,8},{4,12},{8,0},{12,4},{1,9},{5,13},{9,1},{13,5},{2,10},{6,14},... | collective-permute-start | bytes 589832 | tf_op jit(solution)/shard_map/ppermute | solution.py:306
  86.1 3.3 %collective-permute-start.11 = (bf16[256,384]{1,0:T(8,128)(2,1)S(1)}, bf16[256,384]{1,0:T(8,128)(2,1)S(1)}, u32[]{:S(2)}, u32[]{:S(2)}) collective-permute-start(bf16[256,384]{1,0:T(8,128)(2,1)S(1)} %add_1_last.1), channel_id=1, source_target_pairs={{0,4},{4,0},{8,12},{12,8},{1,5},{5,1},{9,13},{13,9},{2,6},{6,2},{1... | collective-permute-start | bytes 589832 | tf_op jit(solution)/shard_map/ppermute | solution.py:306
  89.4 0.1 multiply_convert_fusion
  89.5 0.7 copy.29
  90.3 7.4 %collective-permute-done.18.refs_1_ = bf16[256,384]{1,0:T(8,128)(2,1)S(1)} collective-permute-done((bf16[256,384]{1,0:T(8,128)(2,1)S(1)}, bf16[256,384]{1,0:T(8,128)(2,1)S(1)}, u32[]{:S(2)}, u32[]{:S(2)}) %collective-permute-start.18) | collective-permute-done | bytes 196640 | tf_op jit(solution)/shard_map/ppermute | solution.py:306
  97.7 1.3 %weighted_sum.1 = bf16[256,384]{1,0:T(8,128)(2,1)} custom-call(s32[1]{0:T(128)} %bitcast.10.index_ref, s32[256,2]{1,0:T(8,128)S(1)} %copy.27.id_ref, f32[256,2]{1,0:T(8,128)S(1)} %copy.28.weight_ref, bf16[256,384]{1,0:T(8,128)(2,1)S(1)} %get-tuple-element.20.kept_ref, bf16[256,384]{1,0:T(8,128)(2,1)S(1)} %collective-permute-done.4.came_ref, ...), custom_call_target="tpu_custom_call" | custom-call | flops 786432 | bytes 1183748 | tf_op jit(solution)/shard_map/weighted_sum/pallas_call | solution.py:93
  (63 shorter events, 0.3 us)
Async XLA Ops:
  1.3 1.1 %copy-start.6 = (bf16[256,1536]{1,0:T(8,128)(2,1)S(1)}, bf16[256,1536]{1,0:T(8,128)(2,1)}, u32[]{:S(2)}) copy-start(bf16[256,1536]{1,0:T(8,128)(2,1)} %token_ref.1) | copy-start | bytes 2359300
  2.6 32.4 %collective-permute-start.19 = (bf16[64,1536]{1,0:T(8,128)(2,1)S(1)}, bf16[64,1536]{1,0:T(8,128)(2,1)S(1)}, u32[]{:S(2)}, u32[]{:S(2)}) collective-permute-start(bf16[64,1536]{1,0:T(8,128)(2,1)S(1)} %own_piece.1), channel_id=1, source_target_pairs={{0,12},{4,8},{8,4},{12,0},{1,13},{5,9},{9,5},{13,1},{2,14},{6,10},... | collective-permute-start | bytes 589832 | tf_op jit(solution)/shard_map/ppermute | solution.py:270
  7.8 28.9 %collective-permute-start.12 = (bf16[64,1536]{1,0:T(8,128)(2,1)S(1)}, bf16[64,1536]{1,0:T(8,128)(2,1)}, u32[]{:S(2)}, u32[]{:S(2)}) collective-permute-start(bf16[64,1536]{1,0:T(8,128)(2,1)S(1)} %own_piece.1), channel_id=1, source_target_pairs={{0,8},{4,12},{8,0},{12,4},{1,9},{5,13},{9,1},{13,5},{2,10},{6,14},... | collective-permute-start | bytes 589832 | tf_op jit(solution)/shard_map/ppermute | solution.py:270
  9.5 16.3 %collective-permute-start = (bf16[128,512]{1,0:T(8,128)(2,1)S(1)}, bf16[128,512]{1,0:T(8,128)(2,1)}, u32[]{:S(2)}, u32[]{:S(2)}) collective-permute-start(bf16[128,512]{1,0:T(8,128)(2,1)S(1)} %constant_dynamic-update-slice_fusion), channel_id=1, source_target_pairs={{0,4},{4,0},{8,12},{12,8},{1,5},{5,1},{9,13},{13,9},{2,6},{6,2},{1... | collective-permute-start | bytes 393224 | tf_op jit(solution)/shard_map/ppermute | solution.py:32
  10.1 23.9 %collective-permute-start.1 = (bf16[128,512]{1,0:T(8,128)(2,1)S(1)}, bf16[128,512]{1,0:T(8,128)(2,1)}, u32[]{:S(2)}, u32[]{:S(2)}) collective-permute-start(bf16[128,512]{1,0:T(8,128)(2,1)S(1)} %constant_dynamic-update-slice_fusion), channel_id=1, source_target_pairs={{0,8},{4,12},{8,0},{12,4},{1,9},{5,13},{9,1},{13,5},{2,10},{6,14},... | collective-permute-start | bytes 393224 | tf_op jit(solution)/shard_map/ppermute | solution.py:32
  12.4 21.6 %collective-permute-start.2 = (bf16[128,512]{1,0:T(8,128)(2,1)S(1)}, bf16[128,512]{1,0:T(8,128)(2,1)}, u32[]{:S(2)}, u32[]{:S(2)}) collective-permute-start(bf16[128,512]{1,0:T(8,128)(2,1)S(1)} %constant_dynamic-update-slice_fusion), channel_id=1, source_target_pairs={{0,12},{4,8},{8,4},{12,0},{1,13},{5,9},{9,5},{13,1},{2,14},{6,10},... | collective-permute-start | bytes 393224 | tf_op jit(solution)/shard_map/ppermute | solution.py:32
  13.9 1.7 %copy-start = (bf16[1,1536,768]{2,1,0:T(8,128)(2,1)S(1)}, bf16[1,1536,768]{2,1,0:T(8,128)(2,1)}, u32[]{:S(2)}) copy-start(bf16[1,1536,768]{2,1,0:T(8,128)(2,1)} %param.21) | copy-start | bytes 7077892
  15.6 1.7 %copy-start.2 = (bf16[1,1536,768]{2,1,0:T(8,128)(2,1)S(1)}, bf16[1,1536,768]{2,1,0:T(8,128)(2,1)}, u32[]{:S(2)}) copy-start(bf16[1,1536,768]{2,1,0:T(8,128)(2,1)} %param.22) | copy-start | bytes 7077892
  17.3 1.7 %copy-start.4 = (bf16[1,768,1536]{2,1,0:T(8,128)(2,1)S(1)}, bf16[1,768,1536]{2,1,0:T(8,128)(2,1)}, u32[]{:S(2)}) copy-start(bf16[1,768,1536]{2,1,0:T(8,128)(2,1)} %param.23) | copy-start | bytes 7077892
  18.9 1.1 %copy-start.7 = (bf16[256,1536]{1,0:T(8,128)(2,1)S(1)}, bf16[256,1536]{1,0:T(8,128)(2,1)}, u32[]{:S(2)}) copy-start(bf16[256,1536]{1,0:T(8,128)(2,1)} %token_ref.1) | copy-start | bytes 2359300
  20.1 3.7 %copy-start.18 = (s32[256,2]{0,1:T(2,128)S(1)}, s32[256,2]{0,1:T(2,128)}, u32[]{:S(2)}) copy-start(s32[256,2]{0,1:T(2,128)} %param.18) | copy-start | bytes 6148
  20.1 3.8 %copy-start.19 = (f32[256,2]{0,1:T(2,128)S(1)}, f32[256,2]{0,1:T(2,128)}, u32[]{:S(2)}) copy-start(f32[256,2]{0,1:T(2,128)} %param.19) | copy-start | bytes 6148
  23.0 0.8 copy-start.16
  23.7 25.4 %copy-start.1 = (bf16[1,1536,768]{2,1,0:T(8,128)(2,1)S(1)}, bf16[1,1536,768]{2,1,0:T(8,128)(2,1)}, u32[]{:S(2)}) copy-start(bf16[1,1536,768]{2,1,0:T(8,128)(2,1)} %param.21) | copy-start | bytes 7077892
  25.8 14.5 %collective-permute-start.5 = (bf16[64,1536]{1,0:T(8,128)(2,1)S(1)}, bf16[64,1536]{1,0:T(8,128)(2,1)}, u32[]{:S(2)}, u32[]{:S(2)}) collective-permute-start(bf16[64,1536]{1,0:T(8,128)(2,1)S(1)} %own_piece.1), channel_id=1, source_target_pairs={{0,4},{4,0},{8,12},{12,8},{1,5},{5,1},{9,13},{13,9},{2,6},{6,2},{1... | collective-permute-start | bytes 589832 | tf_op jit(solution)/shard_map/ppermute | solution.py:270
  35.1 12.0 %copy-start.14 = (bf16[64,1536]{1,0:T(8,128)(2,1)}, bf16[64,1536]{1,0:T(8,128)(2,1)S(1)}, u32[]{:S(2)}) copy-start(bf16[64,1536]{1,0:T(8,128)(2,1)S(1)} %collective-permute-done.19.refs_2_) | copy-start | bytes 589828
  35.1 7.3 %collective-permute-start.20 = (bf16[64,1536]{1,0:T(8,128)(2,1)S(1)}, bf16[64,1536]{1,0:T(8,128)(2,1)}, u32[]{:S(2)}, u32[]{:S(2)}) collective-permute-start(bf16[64,1536]{1,0:T(8,128)(2,1)S(1)} %collective-permute-done.19.refs_2_), channel_id=1, source_target_pairs={{0,2},{1,3},{2,0},{3,1},{4,6},{5,7},{6,4},{7,5},{8,10},{9,11},{10,... | collective-permute-start | bytes 589832 | tf_op jit(solution)/shard_map/ppermute | solution.py:285
  36.6 9.1 %collective-permute-start.13 = (bf16[64,1536]{1,0:T(8,128)(2,1)}, bf16[64,1536]{1,0:T(8,128)(2,1)}, u32[]{:S(2)}, u32[]{:S(2)}) collective-permute-start(bf16[64,1536]{1,0:T(8,128)(2,1)} %collective-permute-done.12.refs_2_), channel_id=1, source_target_pairs={{0,2},{1,3},{2,0},{3,1},{4,6},{5,7},{6,4},{7,5},{8,10},{9,11},{10,... | collective-permute-start | bytes 589832 | tf_op jit(solution)/shard_map/ppermute | solution.py:285
  39.8 7.3 %collective-permute-start.21 = (bf16[64,1536]{1,0:T(8,128)(2,1)S(1)}, bf16[64,1536]{1,0:T(8,128)(2,1)S(1)}, u32[]{:S(2)}, u32[]{:S(2)}) collective-permute-start(bf16[64,1536]{1,0:T(8,128)(2,1)S(1)} %collective-permute-done.19.refs_2_), channel_id=1, source_target_pairs={{0,1},{1,0},{2,3},{3,2},{4,5},{5,4},{6,7},{7,6},{8,9},{9,8},{10,11... | collective-permute-start | bytes 589832 | tf_op jit(solution)/shard_map/ppermute | solution.py:285
  39.8 17.1 %collective-permute-start.14 = (bf16[64,1536]{1,0:T(8,128)(2,1)}, bf16[64,1536]{1,0:T(8,128)(2,1)S(1)}, u32[]{:S(2)}, u32[]{:S(2)}) collective-permute-start(bf16[64,1536]{1,0:T(8,128)(2,1)} %collective-permute-done.12.refs_2_), channel_id=1, source_target_pairs={{0,1},{1,0},{2,3},{3,2},{4,5},{5,4},{6,7},{7,6},{8,9},{9,8},{10,11... | collective-permute-start | bytes 589832 | tf_op jit(solution)/shard_map/ppermute | solution.py:285
  40.3 8.3 %collective-permute-start.6 = (bf16[64,1536]{1,0:T(8,128)(2,1)}, bf16[64,1536]{1,0:T(8,128)(2,1)S(1)}, u32[]{:S(2)}, u32[]{:S(2)}) collective-permute-start(bf16[64,1536]{1,0:T(8,128)(2,1)} %collective-permute-done.5.refs_2_), channel_id=1, source_target_pairs={{0,2},{1,3},{2,0},{3,1},{4,6},{5,7},{6,4},{7,5},{8,10},{9,11},{10,... | collective-permute-start | bytes 589832 | tf_op jit(solution)/shard_map/ppermute | solution.py:285
  42.4 6.2 %collective-permute-start.22 = (bf16[64,1536]{1,0:T(8,128)(2,1)}, bf16[64,1536]{1,0:T(8,128)(2,1)S(1)}, u32[]{:S(2)}, u32[]{:S(2)}) collective-permute-start(bf16[64,1536]{1,0:T(8,128)(2,1)} %collective-permute-done.20.refs_3_), channel_id=1, source_target_pairs={{0,1},{1,0},{2,3},{3,2},{4,5},{5,4},{6,7},{7,6},{8,9},{9,8},{10,11... | collective-permute-start | bytes 589832 | tf_op jit(solution)/shard_map/ppermute | solution.py:285
  45.7 11.2 %collective-permute-start.15 = (bf16[64,1536]{1,0:T(8,128)(2,1)}, bf16[64,1536]{1,0:T(8,128)(2,1)S(1)}, u32[]{:S(2)}, u32[]{:S(2)}) collective-permute-start(bf16[64,1536]{1,0:T(8,128)(2,1)} %collective-permute-done.13.refs_3_), channel_id=1, source_target_pairs={{0,1},{1,0},{2,3},{3,2},{4,5},{5,4},{6,7},{7,6},{8,9},{9,8},{10,11... | collective-permute-start | bytes 589832 | tf_op jit(solution)/shard_map/ppermute | solution.py:285
  47.1 18.5 %copy-start.17 = (f32[2,2,128,512]{2,3,1,0:T(8,128)}, f32[2,2,128,512]{2,3,1,0:T(8,128)S(1)}, u32[]{:S(2)}) copy-start(f32[2,2,128,512]{2,3,1,0:T(8,128)S(1)} %get-tuple-element.41) | copy-start | bytes 3145732
  47.1 27.5 %collective-permute-start.3 = (bf16[256,768]{1,0:T(8,128)(2,1)}, bf16[256,768]{1,0:T(8,128)(2,1)S(1)}, u32[]{:S(2)}, u32[]{:S(2)}) collective-permute-start(bf16[256,768]{1,0:T(8,128)(2,1)} %copy-done.16), channel_id=1, source_target_pairs={{0,1},{1,0},{2,3},{3,2},{4,5},{5,4},{6,7},{7,6},{8,9},{9,8},{10,11... | collective-permute-start | bytes 1179656 | tf_op jit(solution)/shard_map/ppermute | solution.py:292
  48.6 12.5 %collective-permute-start.7 = (bf16[64,1536]{1,0:T(8,128)(2,1)}, bf16[64,1536]{1,0:T(8,128)(2,1)S(1)}, u32[]{:S(2)}, u32[]{:S(2)}) collective-permute-start(bf16[64,1536]{1,0:T(8,128)(2,1)} %collective-permute-done.5.refs_2_), channel_id=1, source_target_pairs={{0,1},{1,0},{2,3},{3,2},{4,5},{5,4},{6,7},{7,6},{8,9},{9,8},{10,11... | collective-permute-start | bytes 589832 | tf_op jit(solution)/shard_map/ppermute | solution.py:285
  48.6 12.5 %collective-permute-start.8 = (bf16[64,1536]{1,0:T(8,128)(2,1)S(1)}, bf16[64,1536]{1,0:T(8,128)(2,1)S(1)}, u32[]{:S(2)}, u32[]{:S(2)}) collective-permute-start(bf16[64,1536]{1,0:T(8,128)(2,1)S(1)} %collective-permute-done.6.refs_3_), channel_id=1, source_target_pairs={{0,1},{1,0},{2,3},{3,2},{4,5},{5,4},{6,7},{7,6},{8,9},{9,8},{10,11... | collective-permute-start | bytes 589832 | tf_op jit(solution)/shard_map/ppermute | solution.py:285
  49.1 1.7 %copy-start.3 = (bf16[1,1536,768]{2,1,0:T(8,128)(2,1)S(1)}, bf16[1,1536,768]{2,1,0:T(8,128)(2,1)}, u32[]{:S(2)}) copy-start(bf16[1,1536,768]{2,1,0:T(8,128)(2,1)} %param.22) | copy-start | bytes 7077892
  50.8 1.7 %copy-start.5 = (bf16[1,768,1536]{2,1,0:T(8,128)(2,1)S(1)}, bf16[1,768,1536]{2,1,0:T(8,128)(2,1)}, u32[]{:S(2)}) copy-start(bf16[1,768,1536]{2,1,0:T(8,128)(2,1)} %param.23) | copy-start | bytes 7077892
  52.4 0.9 copy-start.15
  56.9 3.8 %copy-start.8 = (bf16[256,768]{1,0:T(8,128)(2,1)}, bf16[256,768]{1,0:T(8,128)(2,1)S(1)}, u32[]{:S(2)}) copy-start(bf16[256,768]{1,0:T(8,128)(2,1)S(1)} %get-tuple-element.30.kept_ref) | copy-start | bytes 1179652
  56.9 11.6 %collective-permute-start.23 = (bf16[256,768]{1,0:T(8,128)(2,1)}, bf16[256,768]{1,0:T(8,128)(2,1)}, u32[]{:S(2)}, u32[]{:S(2)}) collective-permute-start(bf16[256,768]{1,0:T(8,128)(2,1)} %get-tuple-element.31), channel_id=1, source_target_pairs={{0,1},{1,0},{2,3},{3,2},{4,5},{5,4},{6,7},{7,6},{8,9},{9,8},{10,11... | collective-permute-start | bytes 1179656 | tf_op jit(solution)/shard_map/ppermute | solution.py:292
  60.7 3.9 %copy-start.10 = (bf16[256,768]{1,0:T(8,128)(2,1)}, bf16[256,768]{1,0:T(8,128)(2,1)S(1)}, u32[]{:S(2)}) copy-start(bf16[256,768]{1,0:T(8,128)(2,1)S(1)} %get-tuple-element.26.kept_ref) | copy-start | bytes 1179652
  60.7 10.5 %collective-permute-start.16 = (bf16[256,768]{1,0:T(8,128)(2,1)}, bf16[256,768]{1,0:T(8,128)(2,1)}, u32[]{:S(2)}, u32[]{:S(2)}) collective-permute-start(bf16[256,768]{1,0:T(8,128)(2,1)} %get-tuple-element.27), channel_id=1, source_target_pairs={{0,1},{1,0},{2,3},{3,2},{4,5},{5,4},{6,7},{7,6},{8,9},{9,8},{10,11... | collective-permute-start | bytes 1179656 | tf_op jit(solution)/shard_map/ppermute | solution.py:292
  64.6 0.8 copy-start.12
  65.4 3.0 %copy-start.20 = (f32[2]{0:T(128)S(1)}, f32[2]{0:T(128)}, u32[]{:S(2)}) copy-start(f32[2]{0:T(128)} %param.15) | copy-start | bytes 28
  65.4 3.1 %copy-start.9 = (bf16[256,768]{1,0:T(8,128)(2,1)S(1)}, bf16[256,768]{1,0:T(8,128)(2,1)}, u32[]{:S(2)}) copy-start(bf16[256,768]{1,0:T(8,128)(2,1)} %copy-done.8) | copy-start | bytes 1179652
  65.4 5.8 %copy-start.11 = (bf16[256,768]{1,0:T(8,128)(2,1)S(1)}, bf16[256,768]{1,0:T(8,128)(2,1)}, u32[]{:S(2)}) copy-start(bf16[256,768]{1,0:T(8,128)(2,1)} %copy-done.10) | copy-start | bytes 1179652
  65.4 7.5 %collective-permute-start.9 = (bf16[256,768]{1,0:T(8,128)(2,1)}, bf16[256,768]{1,0:T(8,128)(2,1)S(1)}, u32[]{:S(2)}, u32[]{:S(2)}) collective-permute-start(bf16[256,768]{1,0:T(8,128)(2,1)} %get-tuple-element.23), channel_id=1, source_target_pairs={{0,1},{1,0},{2,3},{3,2},{4,5},{5,4},{6,7},{7,6},{8,9},{9,8},{10,11... | collective-permute-start | bytes 1179656 | tf_op jit(solution)/shard_map/ppermute | solution.py:292
  65.6 7.4 %copy-start.13 = (bf16[256,768]{1,0:T(8,128)(2,1)S(1)}, bf16[256,768]{1,0:T(8,128)(2,1)}, u32[]{:S(2)}) copy-start(bf16[256,768]{1,0:T(8,128)(2,1)} %copy-done.12) | copy-start | bytes 1179652
  68.5 20.9 %copy-start.21 = (f32[128]{0:T(128)S(1)}, f32[128]{0:T(128)}, u32[]{:S(2)}) copy-start(f32[128]{0:T(128)} %param.16) | copy-start | bytes 1540
  69.7 7.8 %collective-permute-start.24 = (bf16[256,384]{1,0:T(8,128)(2,1)S(1)}, bf16[256,384]{1,0:T(8,128)(2,1)S(1)}, u32[]{:S(2)}, u32[]{:S(2)}) collective-permute-start(bf16[256,384]{1,0:T(8,128)(2,1)S(1)} %get-tuple-element.33), channel_id=1, source_target_pairs={{0,2},{1,3},{2,0},{3,1},{4,6},{5,7},{6,4},{7,5},{8,10},{9,11},{10,... | collective-permute-start | bytes 589832 | tf_op jit(solution)/shard_map/ppermute | solution.py:292
  72.3 9.4 %collective-permute-start.17 = (bf16[256,384]{1,0:T(8,128)(2,1)S(1)}, bf16[256,384]{1,0:T(8,128)(2,1)S(1)}, u32[]{:S(2)}, u32[]{:S(2)}) collective-permute-start(bf16[256,384]{1,0:T(8,128)(2,1)S(1)} %get-tuple-element.29), channel_id=1, source_target_pairs={{0,2},{1,3},{2,0},{3,1},{4,6},{5,7},{6,4},{7,5},{8,10},{9,11},{10,... | collective-permute-start | bytes 589832 | tf_op jit(solution)/shard_map/ppermute | solution.py:292
  73.0 13.0 %collective-permute-start.10 = (bf16[256,384]{1,0:T(8,128)(2,1)S(1)}, bf16[256,384]{1,0:T(8,128)(2,1)S(1)}, u32[]{:S(2)}, u32[]{:S(2)}) collective-permute-start(bf16[256,384]{1,0:T(8,128)(2,1)S(1)} %get-tuple-element.25), channel_id=1, source_target_pairs={{0,2},{1,3},{2,0},{3,1},{4,6},{5,7},{6,4},{7,5},{8,10},{9,11},{10,... | collective-permute-start | bytes 589832 | tf_op jit(solution)/shard_map/ppermute | solution.py:292
  74.7 15.6 %collective-permute-start.4 = (bf16[256,384]{1,0:T(8,128)(2,1)S(1)}, bf16[256,384]{1,0:T(8,128)(2,1)S(1)}, u32[]{:S(2)}, u32[]{:S(2)}) collective-permute-start(bf16[256,384]{1,0:T(8,128)(2,1)S(1)} %get-tuple-element.21), channel_id=1, source_target_pairs={{0,2},{1,3},{2,0},{3,1},{4,6},{5,7},{6,4},{7,5},{8,10},{9,11},{10,... | collective-permute-start | bytes 589832 | tf_op jit(solution)/shard_map/ppermute | solution.py:292
  77.6 12.7 %collective-permute-start.25 = (bf16[256,384]{1,0:T(8,128)(2,1)S(1)}, bf16[256,384]{1,0:T(8,128)(2,1)S(1)}, u32[]{:S(2)}, u32[]{:S(2)}) collective-permute-start(bf16[256,384]{1,0:T(8,128)(2,1)S(1)} %add_3_last.1), channel_id=1, source_target_pairs={{0,12},{4,8},{8,4},{12,0},{1,13},{5,9},{9,5},{13,1},{2,14},{6,10},... | collective-permute-start | bytes 589832 | tf_op jit(solution)/shard_map/ppermute | solution.py:306
  81.8 15.9 %collective-permute-start.18 = (bf16[256,384]{1,0:T(8,128)(2,1)S(1)}, bf16[256,384]{1,0:T(8,128)(2,1)S(1)}, u32[]{:S(2)}, u32[]{:S(2)}) collective-permute-start(bf16[256,384]{1,0:T(8,128)(2,1)S(1)} %add_2_last.1), channel_id=1, source_target_pairs={{0,8},{4,12},{8,0},{12,4},{1,9},{5,13},{9,1},{13,5},{2,10},{6,14},... | collective-permute-start | bytes 589832 | tf_op jit(solution)/shard_map/ppermute | solution.py:306
  86.1 11.6 %collective-permute-start.11 = (bf16[256,384]{1,0:T(8,128)(2,1)S(1)}, bf16[256,384]{1,0:T(8,128)(2,1)S(1)}, u32[]{:S(2)}, u32[]{:S(2)}) collective-permute-start(bf16[256,384]{1,0:T(8,128)(2,1)S(1)} %add_1_last.1), channel_id=1, source_target_pairs={{0,4},{4,0},{8,12},{12,8},{1,5},{5,1},{9,13},{13,9},{2,6},{6,2},{1... | collective-permute-start | bytes 589832 | tf_op jit(solution)/shard_map/ppermute | solution.py:306

commit v3 on v0

--- a/solution.py
+++ b/solution.py
@@ -1,7 +1,33 @@
+import math
+
 import jax
 import jax.numpy as jnp
 from jax import lax
+from jax.experimental import pallas as pl
+from jax.experimental.pallas import tpu as pltpu
 from jax.sharding import PartitionSpec as P
+
+
+PREPARE_GRANT = 54 << 20
+LOAD_GRANT = 46 << 20
+
+
+def swap(value, axis, step):
+    size = lax.axis_size(axis)
+    return lax.ppermute(value, axis, [(i, i ^ step) for i in range(size)])
+
+
+def halving_steps(size):
+    steps = []
+    step = size // 2
+    while step >= 1:
+        steps.append(step)
+        step //= 2
+    return steps
+
+
+def power_of_two(size):
+    return size & (size - 1) == 0
 
 
 def attend(queries, keys, values, lambdas, head_gain):
@@ -41,19 +67,416 @@
     )
 
 
-def experts(tokens, route_ids, route_weights, moe_gain, w_gate, w_up, w_down):
+def normalize(tokens, moe_gain):
+    token_float = tokens.astype(jnp.float32)
+    return (
+        token_float
+        * lax.rsqrt(jnp.mean(token_float * token_float, axis=1, keepdims=True) + 1e-06)
+        * moe_gain
+    ).astype(jnp.bfloat16)
+
+
+def rms_rows(token_block, gain_row):
+    token_float = token_block.astype(jnp.float32)
+    scale = lax.rsqrt(jnp.mean(token_float * token_float, axis=1, keepdims=True) + 1e-06)
+    return (token_float * scale * gain_row).astype(jnp.bfloat16)
+
+
+def call(kernel, inputs, spaces, out_shapes, scratch, flops, grant):
+    moved = sum(x.size * x.dtype.itemsize for x in inputs)
+    moved += sum(math.prod(o.shape) * o.dtype.itemsize for o in out_shapes)
+    return kernel_call(kernel, inputs, spaces, out_shapes, scratch, flops, moved, grant)
+
+
+def kernel_call(kernel, inputs, spaces, out_shapes, scratch, flops, moved, grant):
+    return pl.pallas_call(
+        kernel,
+        out_shape=out_shapes,
+        in_specs=[pl.BlockSpec(memory_space=s) for s in spaces],
+        out_specs=[pl.BlockSpec(memory_space=pltpu.VMEM)] * len(out_shapes),
+        scratch_shapes=scratch,
+        cost_estimate=pl.CostEstimate(flops=flops, bytes_accessed=moved, transcendentals=0),
+        compiler_params=pltpu.CompilerParams(vmem_limit_bytes=grant),
+    )(*inputs)
+
+
+def reversed_bits(index, steps):
+    part = jnp.zeros((), jnp.int32)
+    for place, step in enumerate(steps):
+        part = part + jnp.where(index & step != 0, 1 << place, 0)
+    return part
+
+
+def started(pairs, sems):
+    copies = [
+        pltpu.make_async_copy(source, target, sems.at[number])
+        for number, (source, target) in enumerate(pairs)
+    ]
+    for copy in copies:
+        copy.start()
+    return copies
+
+
+def prepare(tokens, moe_gain, keys, values, route_ids, route_weights):
+    row_count, width = tokens.shape
+    top_count = route_ids.shape[1]
+    ep_size = lax.axis_size("ep")
+    tp_size = lax.axis_size("tp")
+    steps = halving_steps(tp_size)[:-1]
+    piece_rows = row_count // tp_size
+    half = row_count // 2
+    key_width = keys.shape[1]
+    lines = -(-ep_size // 128) * 128
+
+    def kernel(token_ref, gain_ref, key_ref, value_ref, id_ref, scale_ref, *refs):
+        piece_ref, half_ref, both_ref, weight_ref, rows, gains, ids, scales, table, sems = refs
+        tp_index, ep_index = lax.axis_index("tp"), lax.axis_index("ep")
+        at = pl.multiple_of((tp_index & 1) * half, half)
+        copies = started(
+            [
+                (token_ref.at[pl.ds(at, half), :], rows),
+                (gain_ref, gains),
+                (id_ref, ids),
+                (scale_ref, scales),
+                (key_ref, both_ref.at[:, :key_width]),
+                (value_ref, both_ref.at[:, key_width:]),
+            ],
+            sems,
+        )
+        for copy in copies[2:4]:
+            copy.wait()
+        table[...] = jnp.zeros_like(table)
+        for step in range(ep_size):
+            expert = ep_index ^ step
+            line = jnp.zeros((1, row_count), jnp.float32)
+            for choice in range(top_count):
+                named = ids[choice : choice + 1, :] == expert
+                line += jnp.where(named, scales[choice : choice + 1, :], 0.0)
+            table[step : step + 1, :] = line
+        weight_ref[...] = table[...].T
+        for copy in copies[:2]:
+            copy.wait()
+        half_ref[...] = rms_rows(rows[...], gains[...].reshape(1, width))
+        own = pl.multiple_of(reversed_bits(tp_index, steps) * piece_rows, piece_rows)
+        piece_ref[...] = half_ref[pl.ds(own, piece_rows), :]
+        for copy in copies[4:]:
+            copy.wait()
+
+    return call(
+        kernel,
+        (tokens, moe_gain, keys, values, route_ids.T, route_weights.T),
+        (pltpu.HBM,) * 6,
+        [
+            jax.ShapeDtypeStruct((piece_rows, width), jnp.bfloat16),
+            jax.ShapeDtypeStruct((half, width), jnp.bfloat16),
+            jax.ShapeDtypeStruct((keys.shape[0], key_width + values.shape[1]), jnp.bfloat16),
+            jax.ShapeDtypeStruct((row_count, lines), jnp.float32),
+        ],
+        [
+            pltpu.VMEM((half, width), jnp.bfloat16),
+            pltpu.VMEM((width,), jnp.float32),
+            pltpu.VMEM((top_count, row_count), jnp.int32),
+            pltpu.VMEM((top_count, row_count), jnp.float32),
+            pltpu.VMEM((lines, row_count), jnp.float32),
+            pltpu.SemaphoreType.DMA((6,)),
+        ],
+        8 * half * width,
+        PREPARE_GRANT,
+    )
+
+
+def load(mats):
+    def kernel(*refs):
+        sources, targets, sems = refs[: len(mats)], refs[len(mats) : -1], refs[-1]
+        for copy in started(list(zip(sources, targets)), sems):
+            copy.wait()
+
+    return call(
+        kernel,
+        tuple(mats),
+        (pltpu.HBM,) * len(mats),
+        [jax.ShapeDtypeStruct(m.shape, m.dtype) for m in mats],
+        [pltpu.SemaphoreType.DMA((len(mats),))],
+        1,
+        LOAD_GRANT,
+    )
+
+
+def expert_kernel(pieces, mats):
+    width, units = mats[0][0].shape
+    tp_size = lax.axis_size("tp")
+    steps = halving_steps(tp_size)[:-1]
+    block_count = tp_size // 2
+    block = width // block_count
+    part_rows = pieces[0].shape[0]
+    row_count = part_rows * len(pieces)
+    half = block_count // 2
+    chunk = math.gcd(units, 256)
+    span = math.gcd(block, 384)
+
+    def kernel(*refs):
+        tp_index = lax.axis_index("tp")
+        piece_refs, rest = refs[: len(pieces)], refs[len(pieces) :]
+        mat_refs, (send_ref, keep_ref, rows, hidden) = rest[:-4], rest[-4:]
+        sets = [mat_refs[i : i + 3] for i in range(0, len(mat_refs), 3)]
+        if len(pieces) == 1:
+            rows[...] = piece_refs[0][...]
+        else:
+            flips = [0]
+            for step in steps:
+                flips = flips + [f ^ step for f in flips]
+            for flip, ref in zip(flips, piece_refs):
+                at = reversed_bits(tp_index ^ flip, steps) * part_rows
+                at = pl.multiple_of(at, part_rows)
+                rows[pl.ds(at, part_rows), :] = ref[...]
+        for number, (gate_ref, up_ref, _) in enumerate(sets):
+            for step in range(units // chunk):
+                columns = pl.ds(step * chunk, chunk)
+                gate = jnp.dot(rows[...], gate_ref[:, columns], preferred_element_type=jnp.float32)
+                upward = jnp.dot(rows[...], up_ref[:, columns], preferred_element_type=jnp.float32)
+                result = gate / (1.0 + jnp.exp(-gate)) * upward
+                hidden[:, pl.ds(number * units + step * chunk, chunk)] = result.astype(jnp.bfloat16)
+        for index in range(block_count):
+            target = send_ref if index < half else keep_ref
+            owner = tp_index >> 1
+            for bit, step in enumerate(steps):
+                if not (index >> bit) & 1:
+                    owner = owner ^ (step >> 1)
+            for step in range(block // span):
+                at = pl.multiple_of(owner * block + step * span, span)
+                out = jnp.zeros((row_count, span), jnp.float32)
+                for number, (_, _, down_ref) in enumerate(sets):
+                    out += jnp.dot(
+                        hidden[:, number * units : (number + 1) * units],
+                        down_ref[:, pl.ds(at, span)],
+                        preferred_element_type=jnp.float32,
+                    )
+                start = (index % half) * block + step * span
+                target[:, start : start + span] = out.astype(jnp.bfloat16)
+
+    flat_mats = tuple(m for group in mats for m in group)
+    inputs = (*pieces, *flat_mats)
+    spaces = (pltpu.VMEM,) * len(inputs)
+    shape = jax.ShapeDtypeStruct((row_count, half * block), jnp.bfloat16)
+    return call(
+        kernel,
+        inputs,
+        spaces,
+        [shape, shape],
+        [
+            pltpu.VMEM((row_count, width), jnp.bfloat16),
+            pltpu.VMEM((row_count, units * len(mats)), jnp.bfloat16),
+        ],
+        6 * row_count * width * units * len(mats),
+        10 << 20,
+    )
+
+
+def add_halves(kept, came):
+    row_count, columns = kept.shape
+    half = columns // 2
+
+    def kernel(kept_ref, came_ref, send_ref, keep_ref):
+        for ref, at in ((send_ref, 0), (keep_ref, half)):
+            one = kept_ref[:, at : at + half].astype(jnp.float32)
+            two = came_ref[:, at : at + half].astype(jnp.float32)
+            ref[...] = (one + two).astype(jnp.bfloat16)
+
+    shape = jax.ShapeDtypeStruct((row_count, half), jnp.bfloat16)
+    return call(
+        kernel, (kept, came), (pltpu.VMEM,) * 2, [shape, shape], [], row_count * columns, 4 << 20
+    )
+
+
+def add_last(kept, came):
+    def kernel(kept_ref, came_ref, out_ref):
+        out_ref[...] = (
+            kept_ref[...].astype(jnp.float32) + came_ref[...].astype(jnp.float32)
+        ).astype(jnp.bfloat16)
+
+    return call(
+        kernel,
+        (kept, came),
+        (pltpu.VMEM,) * 2,
+        [jax.ShapeDtypeStruct(kept.shape, jnp.bfloat16)],
+        [],
+        kept.size,
+        4 << 20,
+    )[0]
+
+
+def weighted_sum(weights, own, results):
+    row_count, columns = results[0].shape
+    half = columns // 2
+
+    def kernel(weight_ref, kept_ref, came_ref, *refs):
+        result_refs, (send_ref, keep_ref) = refs[:-2], refs[-2:]
+        core = lax.axis_index("tp") & 1
+        first = pl.multiple_of(core * row_count, row_count)
+        for ref, side in ((send_ref, 1 - core), (keep_ref, core)):
+            at = pl.multiple_of(side * half, half)
+            total = jnp.zeros((row_count, half), jnp.float32)
+            for step in range(len(results) + 1):
+                weight = weight_ref[pl.ds(first, row_count), step : step + 1]
+                if step == 0:
+                    result = kept_ref[:, pl.ds(at, half)].astype(jnp.float32)
+                    result += came_ref[:, pl.ds(at, half)].astype(jnp.float32)
+                else:
+                    result = result_refs[step - 1][:, pl.ds(at, half)].astype(jnp.float32)
+                total += jnp.where(weight != 0.0, result * weight, 0.0)
+            ref[...] = total.astype(jnp.bfloat16)
+
+    inputs = (weights, *own, *results)
+    shape = jax.ShapeDtypeStruct((row_count, half), jnp.bfloat16)
+    return call(
+        kernel,
+        inputs,
+        (pltpu.VMEM,) * len(inputs),
+        [shape, shape],
+        [],
+        8 * row_count * columns,
+        8 << 20,
+    )
+
+
+def both_halves(kept, came):
+    row_count, columns = kept.shape
+
+    def kernel(kept_ref, came_ref, out_ref):
+        core = lax.axis_index("tp") & 1
+        mine = pl.multiple_of(core * row_count, row_count)
+        other = pl.multiple_of((1 - core) * row_count, row_count)
+        out_ref[pl.ds(mine, row_count), :] = kept_ref[...]
+        out_ref[pl.ds(other, row_count), :] = came_ref[...]
+
+    return call(
+        kernel,
+        (kept, came),
+        (pltpu.VMEM,) * 2,
+        [jax.ShapeDtypeStruct((2 * row_count, columns), jnp.bfloat16)],
+        [],
+        row_count * columns,
+        4 << 20,
+    )[0]
+
+
+def attention(queries, keys, values, others, lambdas, head_gain):
+    row_count, width = queries.shape
+    head_count = lambdas.shape[0]
+    pair = width // head_count
+    head_dim = pair // 2
+    value_dim = values.shape[1] // head_count
+    count = row_count * (len(others) + 1)
+    score_scale = head_dim ** (-0.5)
+
+    def kernel(lambda_ref, gain_ref, query_ref, key_ref, value_ref, *refs):
+        other_refs, (out_ref, all_keys, all_values) = refs[:-3], refs[-3:]
+        all_keys[:row_count, :] = key_ref[...]
+        all_values[:row_count, :] = value_ref[...]
+        for index, ref in enumerate(other_refs):
+            rows = slice((index + 1) * row_count, (index + 2) * row_count)
+            all_keys[rows, :] = ref[:, :width]
+            all_values[rows, :] = ref[:, width:]
+        lane = lax.broadcasted_iota(jnp.int32, (row_count, pair), 1)
+        for head in range(head_count):
+            query = query_ref[:, head * pair : (head + 1) * pair]
+            key = all_keys[:, head * pair : (head + 1) * pair]
+            value = all_values[:, head * value_dim : (head + 1) * value_dim]
+            means = []
+            for part in range(2):
+                here = (lane < head_dim) if part == 0 else (lane >= head_dim)
+                masked = jnp.where(here, query, jnp.zeros_like(query))
+                scores = (
+                    lax.dot_general(
+                        masked, key, (((1,), (1,)), ((), ())), preferred_element_type=jnp.float32
+                    )
+                    * score_scale
+                )
+                raised = jnp.exp(scores - jnp.max(scores, axis=1, keepdims=True))
+                totals = jnp.sum(raised, axis=1, keepdims=True)
+                sums = jnp.dot(
+                    raised.astype(jnp.bfloat16), value, preferred_element_type=jnp.float32
+                )
+                means.append(sums / totals)
+            mixed = means[0] - lambda_ref[head] * means[1]
+            scale = lax.rsqrt(jnp.mean(mixed * mixed, axis=1, keepdims=True) + 1e-06)
+            out_ref[:, head * value_dim : (head + 1) * value_dim] = (
+                mixed * scale * gain_ref[...].reshape(1, value_dim)
+            ).astype(jnp.bfloat16)
+
+    inputs = (lambdas, head_gain, queries, keys, values, *others)
+    return call(
+        kernel,
+        inputs,
+        (pltpu.SMEM,) + (pltpu.VMEM,) * (len(inputs) - 1),
+        [jax.ShapeDtypeStruct((row_count, head_count * value_dim), jnp.bfloat16)],
+        [
+            pltpu.VMEM((count, width), jnp.bfloat16),
+            pltpu.VMEM((count, values.shape[1]), jnp.bfloat16),
+        ],
+        4 * row_count * count * (width + 2 * values.shape[1]),
+        12 << 20,
+    )[0]
+
+
+def whole_rows(
+    queries, keys, values, lambdas, head_gain, tokens, route_ids, route_weights, moe_gain, *mats
+):
+    ep_size = lax.axis_size("ep")
+    tp_size = lax.axis_size("tp")
+    steps = halving_steps(tp_size)[:-1]
+    mine, own_rows, both, weights = prepare(
+        tokens, moe_gain, keys, values, route_ids, route_weights
+    )
+    mats = [m[0] for m in mats]
+    others_mats = [swap(m, "tp", 1) for m in mats]
+    mats = (load(mats), others_mats)
+
+    def gathered(piece):
+        pieces = [piece]
+        for place in range(1, ep_size):
+            low = place & -place
+            pieces.append(swap(pieces[place ^ low], "ep", low))
+        return pieces[1:]
+
+    arrivals = gathered(mine)
+    others = gathered(both)
+
+    def half_rows(piece):
+        pieces = [piece]
+        for step in steps:
+            pieces = pieces + [swap(p, "tp", step) for p in pieces]
+        return pieces
+
+    def reduced(send, keep, last):
+        for step in reversed(steps):
+            came = swap(send, "tp", step)
+            if step == steps[0]:
+                return add_last(keep, came) if last else (keep, came)
+            send, keep = add_halves(keep, came)
+
+    own = expert_kernel([own_rows], mats)
+    own = reduced(*own, False)
+    results = []
+    for step in range(1, ep_size):
+        pieces = half_rows(arrivals[step - 1])
+        done = expert_kernel(pieces, mats)
+        done = reduced(*done, True)
+        results.append(swap(done, "ep", step))
+    heads_out = attention(queries, keys, values, others, lambdas, head_gain)
+    send, keep = weighted_sum(weights, own, results)
+    came = swap(send, "tp", 1)
+    return heads_out, both_halves(keep, came)
+
+
+def experts_slots(tokens, route_ids, route_weights, moe_gain, w_gate, w_up, w_down):
     row_count, width = tokens.shape
     top_count = route_ids.shape[1]
     ep_size = lax.axis_size("ep")
     tp_size = lax.axis_size("tp")
     expert_count = w_gate.shape[0] * ep_size
     capacity = 2 * row_count * top_count // expert_count
-    token_float = tokens.astype(jnp.float32)
-    normed = (
-        token_float
-        * lax.rsqrt(jnp.mean(token_float * token_float, axis=1, keepdims=True) + 1e-06)
-        * moe_gain
-    ).astype(jnp.bfloat16)
+    normed = normalize(tokens, moe_gain)
     flat_ids = route_ids.reshape(-1)
     onehot = (flat_ids[:, None] == jnp.arange(expert_count, dtype=jnp.int32)[None, :]).astype(
         jnp.int32
@@ -95,6 +518,27 @@
     )
     combined = jnp.einsum("drk,rk->rd", picked, route_weights)
     return combined.astype(jnp.bfloat16)
+
+
+def fits_whole(queries, keys, values, lambdas, tokens, route_ids, w_gate):
+    row_count, width = tokens.shape
+    ep_size = lax.axis_size("ep")
+    tp_size = lax.axis_size("tp")
+    expert_count = w_gate.shape[0] * ep_size
+    capacity = 2 * row_count * route_ids.shape[1] // expert_count
+    return (
+        capacity >= row_count
+        and w_gate.shape[0] == 1
+        and power_of_two(ep_size)
+        and power_of_two(tp_size)
+        and tp_size >= 4
+        and row_count % (16 * tp_size) == 0
+        and w_gate.shape[2] % 128 == 0
+        and width % (128 * tp_size) == 0
+        and queries.shape[1] % (128 * lambdas.shape[0]) == 0
+        and values.shape[1] % (128 * lambdas.shape[0]) == 0
+        and keys.shape[0] % 128 == 0
+    )
 
 
 def on_device(
@@ -111,9 +555,11 @@
     w_up,
     w_down,
 ):
+    routed = (tokens, route_ids, route_weights, moe_gain, w_gate, w_up, w_down)
+    if fits_whole(queries, keys, values, lambdas, tokens, route_ids, w_gate):
+        return whole_rows(queries, keys, values, lambdas, head_gain, *routed)
     heads_out = attend(queries, keys, values, lambdas, head_gain)
-    expert_out = experts(tokens, route_ids, route_weights, moe_gain, w_gate, w_up, w_down)
-    return (heads_out, expert_out)
+    return (heads_out, experts_slots(*routed))
 
 
 def solution(mesh):

time: 184 us -> 76.1 us (0.41)
  blocking collectives: 67.5 us -> 0 us
  local copies, waits for them, and re-layouts: 24.9 us -> 0.04 us
  Pallas kernels: 0 us -> 18.3 us
  starting transfers between devices: 4.81 us -> 22.1 us
  matrix products: 17 us -> 0 us
  between operations: 14.3 us -> 0.82 us
  waiting for transfers between devices: 48 us -> 34.8 us
  other arithmetic: 6.72 us -> 0 us
    all_gather x2 -> x0, blocking collectives: 41.2 us -> none  [the longest x1 27.2 us: attend(): value_piece = lax.all_gather(values, 'ep', axis=0, tiled=True)]
    ppermute x0 -> x20, waiting for transfers between devices: none -> 34.8 us  [swap(): return lax.ppermute(value, axis, [(i, i ^ step) for i in range(size)])]
    all_gather x1 -> x0, waiting for transfers between devices: 27.7 us -> none  [experts(): piece = lax.all_gather(arrived, 'tp', axis=2, tiled=True)]
    all_to_all x1 -> x0, blocking collectives: 26.4 us -> none  [experts(): lax.all_to_all(own_columns, 'ep', split_axis=0, concat_axis=0, tiled=True)]
    ppermute x0 -> x20, starting transfers between devices: none -> 22.1 us  [swap(): return lax.ppermute(value, axis, [(i, i ^ step) for i in range(size)])]
    unnamed x3 -> x0, waiting for transfers between devices: 20.3 us -> none
    pallas_call x0 -> x12, Pallas kernels: none -> 18.3 us  [kernel_call(): pl.pallas_call(kernel, out_shape=out_shapes, in_specs=[pl.BlockSpec(memor...]
    dot_general x6 -> x0, matrix products: 17 us -> none  [the longest x1 5.36 us: experts(): jnp.einsum('scd,df->scf', piece, up_mat, preferred_element_type=jnp.float32)]
  transfers between devices with their start and end apart: 3 -> 20, of which waited for: 2 -> 8; matrix products, arithmetic and copies ran while one was open for 5% -> 0% of each run, Pallas kernels for 0% -> 23%
where the time goes in v3:
time: 76.1 us; the launch traced here: 75.9 us
  waiting for transfers between devices  34.8 us (46%)
  starting transfers between devices  22.1 us (29%)
  Pallas kernels  18.3 us (24%)
  between operations  0.82 us (1%)
    ppermute x20, waiting for transfers between devices, swap(): return lax.ppermute(value, axis, [(i, i ^ step) for i in range(size)])  34.8 us
    ppermute x20, starting transfers between devices, swap(): return lax.ppermute(value, axis, [(i, i ^ step) for i in range(size)])  22.1 us
    pallas_call x12, Pallas kernels, kernel_call(): pl.pallas_call(kernel, out_shape=out_shapes, in_specs=[pl.BlockSpec(memor...  18.3 us
  transfers between devices with their start and end apart: 20, of which 8 were waited for; matrix products, arithmetic and copies ran while one was open for 0% of the time, Pallas kernels for 23%

profile of v3, /device:TPU:0, one launch (start us, length us, event | category | flops | bytes accessed | tf_op | source)
XLA Modules:
  0.0 75.9 jit_solution(823153711328563956)
XLA Ops:
  0.6 0.6 collective-permute-start.3
  1.2 0.1 collective-permute-start.4
  1.3 0.4 collective-permute-start.5
  1.7 2.1 %shard_map.131 = (bf16[64,1536]{1,0:T(8,128)(2,1)}, bf16[128,1536]{1,0:T(8,128)(2,1)}, bf16[128,512]{1,0:T(8,128)(2,1)}, f32[256,128]{1,0:T(8,128)}) custom-call(bf16[256,1536]{1,0:T(8,128)(2,1)} %token_ref.1, f32[1536]{0:T(1024)} %gain_ref.2, bf16[128,256]{1,0:T(8,128)(2,1)} %key_ref.3, bf16[128,256]{1,0:T(8,128)(2,1)} %value_ref.3, s32[2,256]{1,0:T(2,128)} %bitcast.11, ...), custom_call_target="tpu_custom_call" | custom-call | flops 1572864 | bytes 1779712 | tf_op jit(solution)/shard_map/pallas_call | solution.py:92
  3.9 2.7 %collective-permute-start.7 = (bf16[64,1536]{1,0:T(8,128)(2,1)}, bf16[64,1536]{1,0:T(8,128)(2,1)S(1)}, u32[]{:S(2)}, u32[]{:S(2)}) collective-permute-start(bf16[64,1536]{1,0:T(8,128)(2,1)} %get-tuple-element.27), channel_id=1, source_target_pairs={{0,4},{4,0},{8,12},{12,8},{1,5},{5,1},{9,13},{13,9},{2,6},{6,2},{1... | collective-permute-start | bytes 589832 | tf_op jit(solution)/shard_map/ppermute | solution.py:17
  6.6 2.6 %collective-permute-start.11 = (bf16[64,1536]{1,0:T(8,128)(2,1)}, bf16[64,1536]{1,0:T(8,128)(2,1)S(1)}, u32[]{:S(2)}, u32[]{:S(2)}) collective-permute-start(bf16[64,1536]{1,0:T(8,128)(2,1)} %get-tuple-element.27), channel_id=1, source_target_pairs={{0,8},{4,12},{8,0},{12,4},{1,9},{5,13},{9,1},{13,5},{2,10},{6,14},... | collective-permute-start | bytes 589832 | tf_op jit(solution)/shard_map/ppermute | solution.py:17
  9.1 7.2 %collective-permute-done.7.refs_0_ = bf16[64,1536]{1,0:T(8,128)(2,1)S(1)} collective-permute-done((bf16[64,1536]{1,0:T(8,128)(2,1)}, bf16[64,1536]{1,0:T(8,128)(2,1)S(1)}, u32[]{:S(2)}, u32[]{:S(2)}) %collective-permute-start.7) | collective-permute-done | bytes 196640 | tf_op jit(solution)/shard_map/ppermute | solution.py:17
  16.3 1.7 %collective-permute-start.8 = (bf16[64,1536]{1,0:T(8,128)(2,1)S(1)}, bf16[64,1536]{1,0:T(8,128)(2,1)S(1)}, u32[]{:S(2)}, u32[]{:S(2)}) collective-permute-start(bf16[64,1536]{1,0:T(8,128)(2,1)S(1)} %collective-permute-done.7.refs_0_), channel_id=1, source_target_pairs={{0,2},{1,3},{2,0},{3,1},{4,6},{5,7},{6,4},{7,5},{8,10},{9,11},{10,... | collective-permute-start | bytes 589832 | tf_op jit(solution)/shard_map/ppermute | solution.py:17
  18.0 0.9 %collective-permute-done.11.refs_0_ = bf16[64,1536]{1,0:T(8,128)(2,1)S(1)} collective-permute-done((bf16[64,1536]{1,0:T(8,128)(2,1)}, bf16[64,1536]{1,0:T(8,128)(2,1)S(1)}, u32[]{:S(2)}, u32[]{:S(2)}) %collective-permute-start.11) | collective-permute-done | bytes 196640 | tf_op jit(solution)/shard_map/ppermute | solution.py:17
  18.9 0.4 collective-permute-start.15
  19.3 3.7 %collective-permute-done.8.refs_1_ = bf16[64,1536]{1,0:T(8,128)(2,1)S(1)} collective-permute-done((bf16[64,1536]{1,0:T(8,128)(2,1)S(1)}, bf16[64,1536]{1,0:T(8,128)(2,1)S(1)}, u32[]{:S(2)}, u32[]{:S(2)}) %collective-permute-start.8) | collective-permute-done | bytes 196640 | tf_op jit(solution)/shard_map/ppermute | solution.py:17
  23.0 1.4 %collective-permute-start.12 = (bf16[64,1536]{1,0:T(8,128)(2,1)S(1)}, bf16[64,1536]{1,0:T(8,128)(2,1)S(1)}, u32[]{:S(2)}, u32[]{:S(2)}) collective-permute-start(bf16[64,1536]{1,0:T(8,128)(2,1)S(1)} %collective-permute-done.11.refs_0_), channel_id=1, source_target_pairs={{0,2},{1,3},{2,0},{3,1},{4,6},{5,7},{6,4},{7,5},{8,10},{9,11},{10,... | collective-permute-start | bytes 589832 | tf_op jit(solution)/shard_map/ppermute | solution.py:17
  24.4 3.1 %shard_map.133 = (bf16[1536,768]{1,0:T(8,128)(2,1)S(1)}, bf16[1536,768]{1,0:T(8,128)(2,1)S(1)}, bf16[768,1536]{1,0:T(8,128)(2,1)S(1)}) custom-call(bf16[1536,768]{1,0:T(8,128)(2,1)} %bitcast.6, bf16[1536,768]{1,0:T(8,128)(2,1)} %bitcast.8, bf16[768,1536]{1,0:T(8,128)(2,1)} %bitcast.10), custom_call_target="tpu_custom_call" | custom-call | flops 1 | bytes 14155776 | tf_op jit(solution)/shard_map/pallas_call | solution.py:92
  27.5 0.0 collective-permute-done.15.refs_0_
  27.5 0.7 collective-permute-start.16
  28.2 0.0 collective-permute-done.3.refs_4_.refs_5_
  28.2 0.0 collective-permute-done.4.refs_5_.refs_6_
  28.2 0.0 collective-permute-done.5.refs_6_.refs_7_
  28.2 2.3 %shard_map.135 = (bf16[128,768]{1,0:T(8,128)(2,1)S(1)}, bf16[128,768]{1,0:T(8,128)(2,1)S(1)}) custom-call(bf16[64,1536]{1,0:T(8,128)(2,1)S(1)} %collective-permute-done.7.refs_0_, bf16[64,1536]{1,0:T(8,128)(2,1)S(1)} %collective-permute-done.8.refs_1_, bf16[1536,768]{1,0:T(8,128)(2,1)S(1)} %get-tuple-element.22.refs_1_.refs_2_, ...), custom_call_target="tpu_custom_call" | custom-call | flops 1811939328 | bytes 14942208 | tf_op jit(solution)/shard_map/pallas_call | solution.py:92
  30.6 1.5 %collective-permute-start.9 = (bf16[128,768]{1,0:T(8,128)(2,1)S(1)}, bf16[128,768]{1,0:T(8,128)(2,1)S(1)}, u32[]{:S(2)}, u32[]{:S(2)}) collective-permute-start(bf16[128,768]{1,0:T(8,128)(2,1)S(1)} %get-tuple-element.29), channel_id=1, source_target_pairs={{0,2},{1,3},{2,0},{3,1},{4,6},{5,7},{6,4},{7,5},{8,10},{9,11},{10,... | collective-permute-start | bytes 589832 | tf_op jit(solution)/shard_map/ppermute | solution.py:17
  32.0 0.0 collective-permute-done.12.refs_1_
  32.0 2.3 %shard_map.137 = (bf16[128,768]{1,0:T(8,128)(2,1)S(1)}, bf16[128,768]{1,0:T(8,128)(2,1)S(1)}) custom-call(bf16[64,1536]{1,0:T(8,128)(2,1)S(1)} %collective-permute-done.11.refs_0_, bf16[64,1536]{1,0:T(8,128)(2,1)S(1)} %collective-permute-done.12.refs_1_, bf16[1536,768]{1,0:T(8,128)(2,1)S(1)} %get-tuple-element.22.refs_1_.refs_2_, ...), custom_call_target="tpu_custom_call" | custom-call | flops 1811939328 | bytes 14942208 | tf_op jit(solution)/shard_map/pallas_call | solution.py:92
  34.3 0.0 copy-start
  34.3 0.7 collective-permute-start.13
  35.0 0.0 collective-permute-done.16.refs_1_
  35.0 2.3 %shard_map.139 = (bf16[128,768]{1,0:T(8,128)(2,1)S(1)}, bf16[128,768]{1,0:T(8,128)(2,1)S(1)}) custom-call(bf16[64,1536]{1,0:T(8,128)(2,1)S(1)} %collective-permute-done.15.refs_0_, bf16[64,1536]{1,0:T(8,128)(2,1)S(1)} %collective-permute-done.16.refs_1_, bf16[1536,768]{1,0:T(8,128)(2,1)S(1)} %get-tuple-element.22.refs_1_.refs_2_, ...), custom_call_target="tpu_custom_call" | custom-call | flops 1811939328 | bytes 14942208 | tf_op jit(solution)/shard_map/pallas_call | solution.py:92
  37.3 1.5 %collective-permute-start.17 = (bf16[128,768]{1,0:T(8,128)(2,1)S(1)}, bf16[128,768]{1,0:T(8,128)(2,1)S(1)}, u32[]{:S(2)}, u32[]{:S(2)}) collective-permute-start(bf16[128,768]{1,0:T(8,128)(2,1)S(1)} %get-tuple-element.33), channel_id=1, source_target_pairs={{0,2},{1,3},{2,0},{3,1},{4,6},{5,7},{6,4},{7,5},{8,10},{9,11},{10,... | collective-permute-start | bytes 589832 | tf_op jit(solution)/shard_map/ppermute | solution.py:17
  38.8 0.0 copy-done
  38.8 0.0 copy-start.7
  38.8 2.3 %shard_map.134 = (bf16[128,768]{1,0:T(8,128)(2,1)S(1)}, bf16[128,768]{1,0:T(8,128)(2,1)S(1)}) custom-call(bf16[128,1536]{1,0:T(8,128)(2,1)S(1)} %copy-done, bf16[1536,768]{1,0:T(8,128)(2,1)S(1)} %get-tuple-element.22.refs_1_.refs_2_, bf16[1536,768]{1,0:T(8,128)(2,1)S(1)} %get-tuple-element.23.refs_2_.refs_3_, ...), custom_call_target="tpu_custom_call" | custom-call | flops 1811939328 | bytes 14942208 | tf_op jit(solution)/shard_map/pallas_call | solution.py:92
  41.1 0.0 copy-start.2
  41.1 0.0 copy-start.3
  41.1 0.0 copy-start.4
  41.1 0.0 copy-start.5
  41.2 0.0 copy-start.6
  41.2 0.7 collective-permute-start.6
  41.9 0.0 collective-permute-done.9.came_ref
  41.9 0.1 collective-permute-start.10
  42.0 1.3 %collective-permute-done.13.came_ref = bf16[128,768]{1,0:T(8,128)(2,1)S(1)} collective-permute-done((bf16[128,768]{1,0:T(8,128)(2,1)S(1)}, bf16[128,768]{1,0:T(8,128)(2,1)S(1)}, u32[]{:S(2)}, u32[]{:S(2)}) %collective-permute-start.13) | collective-permute-done | bytes 196640 | tf_op jit(solution)/shard_map/ppermute | solution.py:17
  43.4 2.1 %collective-permute-start.14 = (bf16[128,768]{1,0:T(8,128)(2,1)S(1)}, bf16[128,768]{1,0:T(8,128)(2,1)S(1)}, u32[]{:S(2)}, u32[]{:S(2)}) collective-permute-start(bf16[128,768]{1,0:T(8,128)(2,1)S(1)} %shard_map.138), channel_id=1, source_target_pairs={{0,8},{4,12},{8,0},{12,4},{1,9},{5,13},{9,1},{13,5},{2,10},{6,14},... | collective-permute-start | bytes 589832 | tf_op jit(solution)/shard_map/ppermute | solution.py:17
  45.4 2.1 %collective-permute-done.17.came_ref = bf16[128,768]{1,0:T(8,128)(2,1)S(1)} collective-permute-done((bf16[128,768]{1,0:T(8,128)(2,1)S(1)}, bf16[128,768]{1,0:T(8,128)(2,1)S(1)}, u32[]{:S(2)}, u32[]{:S(2)}) %collective-permute-start.17) | collective-permute-done | bytes 196640 | tf_op jit(solution)/shard_map/ppermute | solution.py:17
  47.6 2.9 %collective-permute-start.18 = (bf16[128,768]{1,0:T(8,128)(2,1)S(1)}, bf16[128,768]{1,0:T(8,128)(2,1)S(1)}, u32[]{:S(2)}, u32[]{:S(2)}) collective-permute-start(bf16[128,768]{1,0:T(8,128)(2,1)S(1)} %shard_map.140), channel_id=1, source_target_pairs={{0,12},{4,8},{8,4},{12,0},{1,13},{5,9},{9,5},{13,1},{2,14},{6,10},... | collective-permute-start | bytes 589832 | tf_op jit(solution)/shard_map/ppermute | solution.py:17
  50.5 0.0 copy-done.7
  50.5 0.0 collective-permute-start.1
  50.5 15.8 %collective-permute-done.1.refs_1_ = bf16[128,512]{1,0:T(8,128)(2,1)S(1)} collective-permute-done((bf16[128,512]{1,0:T(8,128)(2,1)S(1)}, bf16[128,512]{1,0:T(8,128)(2,1)S(1)}, u32[]{:S(2)}, u32[]{:S(2)}) %collective-permute-start.1) | collective-permute-done | bytes 131104 | tf_op jit(solution)/shard_map/ppermute | solution.py:17
  66.3 0.0 collective-permute-start
  66.3 0.0 collective-permute-done.6.came_ref
  66.3 2.0 %collective-permute-start.2 = (bf16[128,512]{1,0:T(8,128)(2,1)S(1)}, bf16[128,512]{1,0:T(8,128)(2,1)S(1)}, u32[]{:S(2)}, u32[]{:S(2)}) collective-permute-start(bf16[128,512]{1,0:T(8,128)(2,1)S(1)} %collective-permute-done.1.refs_1_), channel_id=1, source_target_pairs={{0,4},{4,0},{8,12},{12,8},{1,5},{5,1},{9,13},{13,9},{2,6},{6,2},{1... | collective-permute-start | bytes 393224 | tf_op jit(solution)/shard_map/ppermute | solution.py:17
  68.3 0.0 collective-permute-done.10.refs_0_
  68.3 0.0 collective-permute-done.14.refs_1_
  68.3 0.0 collective-permute-done.18.refs_2_
  68.4 0.0 copy-done.1
  68.4 0.4 shard_map.141
  68.8 0.1 collective-permute-start.19
  68.9 2.4 %collective-permute-done.refs_0_ = bf16[128,512]{1,0:T(8,128)(2,1)S(1)} collective-permute-done((bf16[128,512]{1,0:T(8,128)(2,1)S(1)}, bf16[128,512]{1,0:T(8,128)(2,1)S(1)}, u32[]{:S(2)}, u32[]{:S(2)}) %collective-permute-start) | collective-permute-done | bytes 131104 | tf_op jit(solution)/shard_map/ppermute | solution.py:17
  71.3 1.4 %collective-permute-done.2.refs_2_ = bf16[128,512]{1,0:T(8,128)(2,1)S(1)} collective-permute-done((bf16[128,512]{1,0:T(8,128)(2,1)S(1)}, bf16[128,512]{1,0:T(8,128)(2,1)S(1)}, u32[]{:S(2)}, u32[]{:S(2)}) %collective-permute-start.2) | collective-permute-done | bytes 131104 | tf_op jit(solution)/shard_map/ppermute | solution.py:17
  72.7 0.0 copy-done.2
  72.7 0.0 copy-done.3
  72.7 0.0 copy-done.4
  72.7 0.0 copy-done.5
  72.7 0.0 copy-done.6
  72.7 2.5 %shard_map.132 = bf16[128,256]{1,0:T(8,128)(2,1)} custom-call(f32[2]{0:T(128)S(1)} %copy-done.5, f32[128]{0:T(128)S(1)} %copy-done.6, bf16[128,256]{1,0:T(8,128)(2,1)S(1)} %copy-done.4, bf16[128,256]{1,0:T(8,128)(2,1)S(1)} %copy-done.2, bf16[128,256]{1,0:T(8,128)(2,1)S(1)} %copy-done.3, bf16[128,512]{1,0:T(8,128)(2,1)S(1)} %collective-permute-done.refs_0_, ...), custom_call_target="tpu_custom_call" | custom-call | flops 201326592 | bytes 655880 | tf_op jit(solution)/shard_map/pallas_call | solution.py:92
  75.2 0.0 collective-permute-done.19.came_ref
  75.2 0.7 shard_map.142
  (4 shorter events, 0.1 us)
Async XLA Ops:
  0.6 27.6 %collective-permute-start.3 = (bf16[1536,768]{1,0:T(8,128)(2,1)}, bf16[1536,768]{1,0:T(8,128)(2,1)S(1)}, u32[]{:S(2)}, u32[]{:S(2)}) collective-permute-start(bf16[1536,768]{1,0:T(8,128)(2,1)} %bitcast.5), channel_id=1, source_target_pairs={{0,1},{1,0},{2,3},{3,2},{4,5},{5,4},{6,7},{7,6},{8,9},{9,8},{10,11... | collective-permute-start | bytes 7077896 | tf_op jit(solution)/shard_map/ppermute | solution.py:17
  1.2 27.1 %collective-permute-start.4 = (bf16[1536,768]{1,0:T(8,128)(2,1)}, bf16[1536,768]{1,0:T(8,128)(2,1)S(1)}, u32[]{:S(2)}, u32[]{:S(2)}) collective-permute-start(bf16[1536,768]{1,0:T(8,128)(2,1)} %bitcast.7), channel_id=1, source_target_pairs={{0,1},{1,0},{2,3},{3,2},{4,5},{5,4},{6,7},{7,6},{8,9},{9,8},{10,11... | collective-permute-start | bytes 7077896 | tf_op jit(solution)/shard_map/ppermute | solution.py:17
  1.3 27.0 %collective-permute-start.5 = (bf16[768,1536]{1,0:T(8,128)(2,1)}, bf16[768,1536]{1,0:T(8,128)(2,1)S(1)}, u32[]{:S(2)}, u32[]{:S(2)}) collective-permute-start(bf16[768,1536]{1,0:T(8,128)(2,1)} %bitcast.9), channel_id=1, source_target_pairs={{0,1},{1,0},{2,3},{3,2},{4,5},{5,4},{6,7},{7,6},{8,9},{9,8},{10,11... | collective-permute-start | bytes 7077896 | tf_op jit(solution)/shard_map/ppermute | solution.py:17
  3.9 12.5 %collective-permute-start.7 = (bf16[64,1536]{1,0:T(8,128)(2,1)}, bf16[64,1536]{1,0:T(8,128)(2,1)S(1)}, u32[]{:S(2)}, u32[]{:S(2)}) collective-permute-start(bf16[64,1536]{1,0:T(8,128)(2,1)} %get-tuple-element.27), channel_id=1, source_target_pairs={{0,4},{4,0},{8,12},{12,8},{1,5},{5,1},{9,13},{13,9},{2,6},{6,2},{1... | collective-permute-start | bytes 589832 | tf_op jit(solution)/shard_map/ppermute | solution.py:17
  6.6 12.3 %collective-permute-start.11 = (bf16[64,1536]{1,0:T(8,128)(2,1)}, bf16[64,1536]{1,0:T(8,128)(2,1)S(1)}, u32[]{:S(2)}, u32[]{:S(2)}) collective-permute-start(bf16[64,1536]{1,0:T(8,128)(2,1)} %get-tuple-element.27), channel_id=1, source_target_pairs={{0,8},{4,12},{8,0},{12,4},{1,9},{5,13},{9,1},{13,5},{2,10},{6,14},... | collective-permute-start | bytes 589832 | tf_op jit(solution)/shard_map/ppermute | solution.py:17
  16.3 6.7 %collective-permute-start.8 = (bf16[64,1536]{1,0:T(8,128)(2,1)S(1)}, bf16[64,1536]{1,0:T(8,128)(2,1)S(1)}, u32[]{:S(2)}, u32[]{:S(2)}) collective-permute-start(bf16[64,1536]{1,0:T(8,128)(2,1)S(1)} %collective-permute-done.7.refs_0_), channel_id=1, source_target_pairs={{0,2},{1,3},{2,0},{3,1},{4,6},{5,7},{6,4},{7,5},{8,10},{9,11},{10,... | collective-permute-start | bytes 589832 | tf_op jit(solution)/shard_map/ppermute | solution.py:17
  18.9 8.6 %collective-permute-start.15 = (bf16[64,1536]{1,0:T(8,128)(2,1)S(1)}, bf16[64,1536]{1,0:T(8,128)(2,1)S(1)}, u32[]{:S(2)}, u32[]{:S(2)}) collective-permute-start(bf16[64,1536]{1,0:T(8,128)(2,1)S(1)} %collective-permute-done.11.refs_0_), channel_id=1, source_target_pairs={{0,4},{4,0},{8,12},{12,8},{1,5},{5,1},{9,13},{13,9},{2,6},{6,2},{1... | collective-permute-start | bytes 589832 | tf_op jit(solution)/shard_map/ppermute | solution.py:17
  23.0 9.0 %collective-permute-start.12 = (bf16[64,1536]{1,0:T(8,128)(2,1)S(1)}, bf16[64,1536]{1,0:T(8,128)(2,1)S(1)}, u32[]{:S(2)}, u32[]{:S(2)}) collective-permute-start(bf16[64,1536]{1,0:T(8,128)(2,1)S(1)} %collective-permute-done.11.refs_0_), channel_id=1, source_target_pairs={{0,2},{1,3},{2,0},{3,1},{4,6},{5,7},{6,4},{7,5},{8,10},{9,11},{10,... | collective-permute-start | bytes 589832 | tf_op jit(solution)/shard_map/ppermute | solution.py:17
  27.5 7.5 %collective-permute-start.16 = (bf16[64,1536]{1,0:T(8,128)(2,1)S(1)}, bf16[64,1536]{1,0:T(8,128)(2,1)S(1)}, u32[]{:S(2)}, u32[]{:S(2)}) collective-permute-start(bf16[64,1536]{1,0:T(8,128)(2,1)S(1)} %collective-permute-done.15.refs_0_), channel_id=1, source_target_pairs={{0,2},{1,3},{2,0},{3,1},{4,6},{5,7},{6,4},{7,5},{8,10},{9,11},{10,... | collective-permute-start | bytes 589832 | tf_op jit(solution)/shard_map/ppermute | solution.py:17
  30.6 11.3 %collective-permute-start.9 = (bf16[128,768]{1,0:T(8,128)(2,1)S(1)}, bf16[128,768]{1,0:T(8,128)(2,1)S(1)}, u32[]{:S(2)}, u32[]{:S(2)}) collective-permute-start(bf16[128,768]{1,0:T(8,128)(2,1)S(1)} %get-tuple-element.29), channel_id=1, source_target_pairs={{0,2},{1,3},{2,0},{3,1},{4,6},{5,7},{6,4},{7,5},{8,10},{9,11},{10,... | collective-permute-start | bytes 589832 | tf_op jit(solution)/shard_map/ppermute | solution.py:17
  34.3 4.5 %copy-start = (bf16[128,1536]{1,0:T(8,128)(2,1)S(1)}, bf16[128,1536]{1,0:T(8,128)(2,1)}, u32[]{:S(2)}) copy-start(bf16[128,1536]{1,0:T(8,128)(2,1)} %get-tuple-element.21.refs_0_) | copy-start | bytes 1179652
  34.3 9.0 %collective-permute-start.13 = (bf16[128,768]{1,0:T(8,128)(2,1)S(1)}, bf16[128,768]{1,0:T(8,128)(2,1)S(1)}, u32[]{:S(2)}, u32[]{:S(2)}) collective-permute-start(bf16[128,768]{1,0:T(8,128)(2,1)S(1)} %get-tuple-element.31), channel_id=1, source_target_pairs={{0,2},{1,3},{2,0},{3,1},{4,6},{5,7},{6,4},{7,5},{8,10},{9,11},{10,... | collective-permute-start | bytes 589832 | tf_op jit(solution)/shard_map/ppermute | solution.py:17
  37.3 10.2 %collective-permute-start.17 = (bf16[128,768]{1,0:T(8,128)(2,1)S(1)}, bf16[128,768]{1,0:T(8,128)(2,1)S(1)}, u32[]{:S(2)}, u32[]{:S(2)}) collective-permute-start(bf16[128,768]{1,0:T(8,128)(2,1)S(1)} %get-tuple-element.33), channel_id=1, source_target_pairs={{0,2},{1,3},{2,0},{3,1},{4,6},{5,7},{6,4},{7,5},{8,10},{9,11},{10,... | collective-permute-start | bytes 589832 | tf_op jit(solution)/shard_map/ppermute | solution.py:17
  38.8 11.7 %copy-start.7 = (bf16[128,512]{1,0:T(8,128)(2,1)S(1)}, bf16[128,512]{1,0:T(8,128)(2,1)}, u32[]{:S(2)}) copy-start(bf16[128,512]{1,0:T(8,128)(2,1)} %get-tuple-element.19) | copy-start | bytes 393220
  38.8 29.5 %copy-start.1 = (f32[256,128]{1,0:T(8,128)S(1)}, f32[256,128]{1,0:T(8,128)}, u32[]{:S(2)}) copy-start(f32[256,128]{1,0:T(8,128)} %get-tuple-element.20.weight_ref) | copy-start | bytes 393220
  41.1 31.6 %copy-start.2 = (bf16[128,256]{1,0:T(8,128)(2,1)S(1)}, bf16[128,256]{1,0:T(8,128)(2,1)}, u32[]{:S(2)}) copy-start(bf16[128,256]{1,0:T(8,128)(2,1)} %key_ref.3) | copy-start | bytes 196612
  41.1 31.6 %copy-start.3 = (bf16[128,256]{1,0:T(8,128)(2,1)S(1)}, bf16[128,256]{1,0:T(8,128)(2,1)}, u32[]{:S(2)}) copy-start(bf16[128,256]{1,0:T(8,128)(2,1)} %value_ref.3) | copy-start | bytes 196612
  41.1 31.6 %copy-start.4 = (bf16[128,256]{1,0:T(8,128)(2,1)S(1)}, bf16[128,256]{1,0:T(8,128)(2,1)}, u32[]{:S(2)}) copy-start(bf16[128,256]{1,0:T(8,128)(2,1)} %query_ref.1) | copy-start | bytes 196612
  41.1 31.5 %copy-start.5 = (f32[2]{0:T(128)S(1)}, f32[2]{0:T(128)}, u32[]{:S(2)}) copy-start(f32[2]{0:T(128)} %lambda_ref.1) | copy-start | bytes 28
  41.2 31.5 %copy-start.6 = (f32[128]{0:T(128)S(1)}, f32[128]{0:T(128)}, u32[]{:S(2)}) copy-start(f32[128]{0:T(128)} %gain_ref.3) | copy-start | bytes 1540
  41.2 25.1 %collective-permute-start.6 = (bf16[128,768]{1,0:T(8,128)(2,1)S(1)}, bf16[128,768]{1,0:T(8,128)(2,1)S(1)}, u32[]{:S(2)}, u32[]{:S(2)}) collective-permute-start(bf16[128,768]{1,0:T(8,128)(2,1)S(1)} %get-tuple-element.26), channel_id=1, source_target_pairs={{0,2},{1,3},{2,0},{3,1},{4,6},{5,7},{6,4},{7,5},{8,10},{9,11},{10,... | collective-permute-start | bytes 589832 | tf_op jit(solution)/shard_map/ppermute | solution.py:17
  41.9 26.4 %collective-permute-start.10 = (bf16[128,768]{1,0:T(8,128)(2,1)S(1)}, bf16[128,768]{1,0:T(8,128)(2,1)S(1)}, u32[]{:S(2)}, u32[]{:S(2)}) collective-permute-start(bf16[128,768]{1,0:T(8,128)(2,1)S(1)} %shard_map.136), channel_id=1, source_target_pairs={{0,4},{4,0},{8,12},{12,8},{1,5},{5,1},{9,13},{13,9},{2,6},{6,2},{1... | collective-permute-start | bytes 589832 | tf_op jit(solution)/shard_map/ppermute | solution.py:17
  43.4 25.0 %collective-permute-start.14 = (bf16[128,768]{1,0:T(8,128)(2,1)S(1)}, bf16[128,768]{1,0:T(8,128)(2,1)S(1)}, u32[]{:S(2)}, u32[]{:S(2)}) collective-permute-start(bf16[128,768]{1,0:T(8,128)(2,1)S(1)} %shard_map.138), channel_id=1, source_target_pairs={{0,8},{4,12},{8,0},{12,4},{1,9},{5,13},{9,1},{13,5},{2,10},{6,14},... | collective-permute-start | bytes 589832 | tf_op jit(solution)/shard_map/ppermute | solution.py:17
  47.6 20.8 %collective-permute-start.18 = (bf16[128,768]{1,0:T(8,128)(2,1)S(1)}, bf16[128,768]{1,0:T(8,128)(2,1)S(1)}, u32[]{:S(2)}, u32[]{:S(2)}) collective-permute-start(bf16[128,768]{1,0:T(8,128)(2,1)S(1)} %shard_map.140), channel_id=1, source_target_pairs={{0,12},{4,8},{8,4},{12,0},{1,13},{5,9},{9,5},{13,1},{2,14},{6,10},... | collective-permute-start | bytes 589832 | tf_op jit(solution)/shard_map/ppermute | solution.py:17
  50.5 15.8 %collective-permute-start.1 = (bf16[128,512]{1,0:T(8,128)(2,1)S(1)}, bf16[128,512]{1,0:T(8,128)(2,1)S(1)}, u32[]{:S(2)}, u32[]{:S(2)}) collective-permute-start(bf16[128,512]{1,0:T(8,128)(2,1)S(1)} %copy-done.7), channel_id=1, source_target_pairs={{0,8},{4,12},{8,0},{12,4},{1,9},{5,13},{9,1},{13,5},{2,10},{6,14},... | collective-permute-start | bytes 393224 | tf_op jit(solution)/shard_map/ppermute | solution.py:17
  66.3 5.0 %collective-permute-start = (bf16[128,512]{1,0:T(8,128)(2,1)S(1)}, bf16[128,512]{1,0:T(8,128)(2,1)S(1)}, u32[]{:S(2)}, u32[]{:S(2)}) collective-permute-start(bf16[128,512]{1,0:T(8,128)(2,1)S(1)} %copy-done.7), channel_id=1, source_target_pairs={{0,4},{4,0},{8,12},{12,8},{1,5},{5,1},{9,13},{13,9},{2,6},{6,2},{1... | collective-permute-start | bytes 393224 | tf_op jit(solution)/shard_map/ppermute | solution.py:17
  66.3 6.4 %collective-permute-start.2 = (bf16[128,512]{1,0:T(8,128)(2,1)S(1)}, bf16[128,512]{1,0:T(8,128)(2,1)S(1)}, u32[]{:S(2)}, u32[]{:S(2)}) collective-permute-start(bf16[128,512]{1,0:T(8,128)(2,1)S(1)} %collective-permute-done.1.refs_1_), channel_id=1, source_target_pairs={{0,4},{4,0},{8,12},{12,8},{1,5},{5,1},{9,13},{13,9},{2,6},{6,2},{1... | collective-permute-start | bytes 393224 | tf_op jit(solution)/shard_map/ppermute | solution.py:17
  68.8 6.5 %collective-permute-start.19 = (bf16[128,384]{1,0:T(8,128)(2,1)S(1)}, bf16[128,384]{1,0:T(8,128)(2,1)S(1)}, u32[]{:S(2)}, u32[]{:S(2)}) collective-permute-start(bf16[128,384]{1,0:T(8,128)(2,1)S(1)} %get-tuple-element.35), channel_id=1, source_target_pairs={{0,1},{1,0},{2,3},{3,2},{4,5},{5,4},{6,7},{7,6},{8,9},{9,8},{10,11... | collective-permute-start | bytes 294920 | tf_op jit(solution)/shard_map/ppermute | solution.py:17
